TPU v7x, 768 devices: a whole 4x8x12 slice. The times are simulated.
768 devices in a mesh: sp: 16 (over y, core), dp: 48 (over z, x).
Axes of the slice: x: 4, y: 8, z: 12, core: 2. Of those that a mesh axis runs over, the one named last changes fastest.
Arguments:
- queries: bfloat16 [48, 4096, 1024], P('dp', 'sp'), may hold values from -250 to 250
- keys: bfloat16 [48, 4096, 1024], P('dp', 'sp'), may hold values from -6 to 6
- values: bfloat16 [48, 4096, 1024], P('dp', 'sp'), may hold values from -6 to 6
- cum_gate: float32 [48, 16, 4096], P('dp', 'sp'), may hold values from -4096 to 0, as said below
- out_weight: bfloat16 [1024, 2112], P(None, 'dp'), may hold values from -1.5 to 1.5
Outputs:
- mixed: bfloat16 [48, 4096, 2112], P('dp', 'sp')
Inputs may be any that keep to these rules, and one draw needn't show every extreme that they name: `cum_gate`: within each head the entries do not rise along positions.
All inputs are finite; a program needn't handle non-finite values.
Results may differ from a plain program's by a relative error of at most 0.0053.
Values may be sent and summed in bfloat16 or wider, within the bound.
No kernel may reach another device: no remote copies, remote signals or barrier semaphores. Data moves between devices by JAX's collectives and lax.ppermute only.
A program may use at most 64 MiB of HBM per device.

v0:
```python
import jax
import jax.numpy as jnp
from jax import lax
from jax.sharding import Mesh
from jax.sharding import PartitionSpec as P

SP = ("sp_0", "sp_1")


def side_by_side(arrays, axis, split_dim, concat_dim, along):
    both = jnp.concatenate(arrays, axis=along)
    out, at, finished = (
        lax.all_to_all(both, axis, split_axis=split_dim, concat_axis=concat_dim, tiled=True),
        0,
        [],
    )
    for a in arrays:
        finished.append(lax.slice_in_dim(out, at, at + a.shape[along], axis=along))
        at += a.shape[along]
    return tuple(finished)


def cut_along(array, dim, count):
    shape = array.shape
    pieces = array.reshape(*shape[:dim], count, shape[dim] // count, *shape[dim + 1 :])
    return jnp.moveaxis(pieces, dim, 0)


def laid_out(pieces, dim):
    shape = list(pieces.shape[1:])
    shape[dim] *= pieces.shape[0]
    return jnp.moveaxis(pieces, 0, dim).reshape(shape)


def turned_blocks(pieces, axes, sequence):
    shape = [lax.axis_size(a) for a in axes]
    pieces = pieces.reshape(*shape, *pieces.shape[1:])
    for k in sequence:
        pieces = lax.all_to_all(pieces, axes[k], split_axis=k, concat_axis=k, tiled=True)
    return pieces.reshape(-1, *pieces.shape[len(axes) :])


def exchange_by_axis(array, axes, sequence, split_dim, concat_dim):
    pieces = cut_along(array, split_dim, lax.axis_size(axes))
    return laid_out(turned_blocks(pieces, axes, sequence), concat_dim)


def attend(query_all, key_all, value_all, gate_all):
    length, width = query_all.shape
    heads = gate_all.shape[0]
    depth = width // heads
    block_rows = min(512, length)
    block_count = length // block_rows
    score_scale = depth ** (-0.5)
    query_blocks = query_all.reshape(block_count, block_rows, heads, depth)
    key_blocks = key_all.reshape(block_count, block_rows, heads, depth)
    value_blocks = value_all.reshape(block_count, block_rows, heads, depth)
    gate_blocks = gate_all.reshape(heads, block_count, block_rows).transpose(1, 0, 2)
    offsets = jnp.arange(block_rows, dtype=jnp.int32)

    def one_block(block_index):
        query_part = lax.dynamic_index_in_dim(query_blocks, block_index, 0, keepdims=False)
        gate_part = lax.dynamic_index_in_dim(gate_blocks, block_index, 0, keepdims=False)
        query_rows = block_index * block_rows + offsets

        def key_step(key_block, carry):
            running_max, running_sum, weighted = carry
            key_part = lax.dynamic_index_in_dim(key_blocks, key_block, 0, keepdims=False)
            value_part = lax.dynamic_index_in_dim(value_blocks, key_block, 0, keepdims=False)
            gate_keys = lax.dynamic_index_in_dim(gate_blocks, key_block, 0, keepdims=False)
            logits = (
                jnp.einsum("qhe,khe->hqk", query_part, key_part, preferred_element_type=jnp.float32)
                * score_scale
            )
            logits = logits + gate_part[:, :, None] - gate_keys[:, None, :]
            key_rows = key_block * block_rows + offsets
            allowed = key_rows[None, :] <= query_rows[:, None]
            logits = jnp.where(allowed[None], logits, -jnp.inf)
            new_max = jnp.maximum(running_max, jnp.max(logits, axis=-1))
            scores = jnp.exp(logits - new_max[..., None])
            factor = jnp.exp(running_max - new_max)
            running_sum = running_sum * factor + jnp.sum(scores, axis=-1)
            weighted = weighted * factor[..., None] + jnp.einsum(
                "hqk,khe->hqe",
                scores.astype(jnp.bfloat16),
                value_part,
                preferred_element_type=jnp.float32,
            )
            return (new_max, running_sum, weighted)

        start_state = (
            jnp.full((heads, block_rows), -jnp.inf, jnp.float32),
            jnp.zeros((heads, block_rows), jnp.float32),
            jnp.zeros((heads, block_rows, depth), jnp.float32),
        )
        final_max, final_sum, weighted = lax.fori_loop(0, block_index + 1, key_step, start_state)
        result = weighted / final_sum[..., None]
        return result.transpose(1, 0, 2).astype(jnp.bfloat16)

    outputs = lax.map(one_block, jnp.arange(block_count, dtype=jnp.int32))
    return outputs.reshape(length, width)


def body(queries, keys, values, cum_gate, out_weight):
    query_heads, key_heads, value_heads = side_by_side((queries, keys, values), SP, 2, 1, 0)
    local_out = attend(query_heads[0], key_heads[0], value_heads[0], cum_gate[0])
    attended = exchange_by_axis(local_out[None], SP, (1, 0), 1, 2)[0]
    whole_weight = lax.all_gather(out_weight, "dp", axis=1, tiled=True)
    mixed = jnp.dot(attended, whole_weight, preferred_element_type=jnp.float32)
    return mixed.astype(jnp.bfloat16)[None]


def solution(mesh):
    split = Mesh(mesh.devices.reshape(8, 2, mesh.shape["dp"]), ("sp_0", "sp_1", "dp"))
    return jax.shard_map(
        body,
        mesh=split,
        in_specs=(
            P("dp", SP, None),
            P("dp", SP, None),
            P("dp", SP, None),
            P("dp", SP, None),
            P(None, "dp"),
        ),
        out_specs=P("dp", SP, None),
        check_vma=False,
    )
```

profile of v0, /device:TPU:1, one launch (start us, length us, event | category | flops | bytes accessed | tf_op | source)
XLA Modules:
  0.0 228.8 jit_solution(1165256074676447269)
XLA Ops:
  6.5 2.5 %copy.24 = bf16[1,256,1024]{1,0,2:T(2,128)(2,1)S(1)} copy(bf16[1,256,1024]{2,1,0:T(8,128)(2,1)} %param.9) | data formatting | bytes 1048576 | tf_op args[0]
  9.0 2.4 %copy.25 = bf16[1,256,1024]{1,0,2:T(2,128)(2,1)S(1)} copy(bf16[1,256,1024]{2,1,0:T(8,128)(2,1)} %param.10) | data formatting | bytes 1048576 | tf_op args[1]
  11.4 2.0 copy.26
  13.4 5.7 %pad_maximum_fusion = bf16[3,256,1024]{1,0,2:T(4,128)(2,1)} fusion(bf16[1,256,1024]{1,0,2:T(2,128)(2,1)} %copy.26, bf16[1,256,1024]{1,0,2:T(2,128)(2,1)S(1)} %copy.25, bf16[1,256,1024]{1,0,2:T(2,128)(2,1)S(1)} %copy.24), kind=kLoop, calls=%fused_computation.30 | loop fusion | flops 4718592 | bytes 3145728 | tf_op jit(solution)/shard_map/concatenate | solution.py:11
  19.1 14.0 %all-to-all-start = ((bf16[3,256,1024]{1,0,2:T(4,128)(2,1)}), bf16[3,256,1024]{1,0,2:T(4,128)(2,1)S(1)}, u32[]{:S(2)}, u32[]{:S(2)}) async-start(bf16[3,256,1024]{1,0,2:T(4,128)(2,1)} %pad_maximum_fusion), calls=%async_computation | async-start | bytes 4194304 | tf_op jit(solution)/shard_map/all_to_all | solution.py:13
  33.1 0.7 all-gather.3.cloned.1.call-update
  33.8 48.4 %all-to-all-done = bf16[3,256,1024]{1,0,2:T(4,128)(2,1)S(1)} async-done(((bf16[3,256,1024]{1,0,2:T(4,128)(2,1)}), bf16[3,256,1024]{1,0,2:T(4,128)(2,1)S(1)}, u32[]{:S(2)}, u32[]{:S(2)}) %all-to-all-start) | async-done | bytes 1572896 | tf_op jit(solution)/shard_map/all_to_all | solution.py:13
  84.4 100.2 %while.29 = (s32[]{:T(128)}, bf16[8,512,1,64]{1,3,2,0:T(8,128)(2,1)S(1)}, s32[8]{0:T(128)S(1)}, bf16[8,512,1,64]{1,3,2,0:T(8,128)(2,1)S(1)}, f32[8,1,512]{2,1,0:...) while((s32[]{:T(128)}, ...), condition=%wide.region_5.6_spmd.clone.clone, body=%wide.region_0.5_spmd.clone.clone.sunk | while | flops 69863432 | bytes 4127322 | solution.py:100
  87.2 0.7 dynamic-slice_bitcast_fusion.5
  89.3 1.7 while.30
  89.3 0.7 constant_dynamic-slice_fusion.2
  93.7 0.7 dynamic-slice_bitcast_fusion.5
  95.9 3.4 %while.30 = (s32[]{:T(128)}, f32[1,512]{1,0:T(1,128)S(1)}, f32[1,512]{1,0:T(1,128)S(1)}, f32[1,512,64]{1,2,0:T(8,128)S(1)}, s32[]{:T(128)}, /*index=5*/s32[512]{...) while((s32[]{:T(128)}, f32[1,512]{1,0:T(1,128)S(1)}, ...), condition=%wide.region_4.4_spmd, body=%wide.region_1.3_spmd.sunk | while | flops 69797376 | bytes 3653843 | solution.py:96
  95.9 0.7 constant_dynamic-slice_fusion.2
  97.6 0.7 constant_dynamic-slice_fusion.2
  102.0 0.7 dynamic-slice_bitcast_fusion.5
  104.1 5.1 %while.30 = (s32[]{:T(128)}, f32[1,512]{1,0:T(1,128)S(1)}, f32[1,512]{1,0:T(1,128)S(1)}, f32[1,512,64]{1,2,0:T(8,128)S(1)}, s32[]{:T(128)}, /*index=5*/s32[512]{...) while((s32[]{:T(128)}, f32[1,512]{1,0:T(1,128)S(1)}, ...), condition=%wide.region_4.4_spmd, body=%wide.region_1.3_spmd.sunk | while | flops 69797376 | bytes 3653843 | solution.py:96
  104.2 0.7 constant_dynamic-slice_fusion.2
  105.9 0.7 constant_dynamic-slice_fusion.2
  107.6 0.7 constant_dynamic-slice_fusion.2
  112.0 0.7 dynamic-slice_bitcast_fusion.5
  114.1 6.8 %while.30 = (s32[]{:T(128)}, f32[1,512]{1,0:T(1,128)S(1)}, f32[1,512]{1,0:T(1,128)S(1)}, f32[1,512,64]{1,2,0:T(8,128)S(1)}, s32[]{:T(128)}, /*index=5*/s32[512]{...) while((s32[]{:T(128)}, f32[1,512]{1,0:T(1,128)S(1)}, ...), condition=%wide.region_4.4_spmd, body=%wide.region_1.3_spmd.sunk | while | flops 69797376 | bytes 3653843 | solution.py:96
  114.1 0.7 constant_dynamic-slice_fusion.2
  115.8 0.7 constant_dynamic-slice_fusion.2
  117.5 0.7 constant_dynamic-slice_fusion.2
  119.2 0.7 constant_dynamic-slice_fusion.2
  123.7 0.7 dynamic-slice_bitcast_fusion.5
  125.8 8.5 %while.30 = (s32[]{:T(128)}, f32[1,512]{1,0:T(1,128)S(1)}, f32[1,512]{1,0:T(1,128)S(1)}, f32[1,512,64]{1,2,0:T(8,128)S(1)}, s32[]{:T(128)}, /*index=5*/s32[512]{...) while((s32[]{:T(128)}, f32[1,512]{1,0:T(1,128)S(1)}, ...), condition=%wide.region_4.4_spmd, body=%wide.region_1.3_spmd.sunk | while | flops 69797376 | bytes 3653843 | solution.py:96
  125.8 0.7 constant_dynamic-slice_fusion.2
  127.5 0.7 constant_dynamic-slice_fusion.2
  129.2 0.7 constant_dynamic-slice_fusion.2
  130.9 0.7 constant_dynamic-slice_fusion.2
  132.6 0.7 constant_dynamic-slice_fusion.2
  137.0 0.7 dynamic-slice_bitcast_fusion.5
  139.2 10.2 %while.30 = (s32[]{:T(128)}, f32[1,512]{1,0:T(1,128)S(1)}, f32[1,512]{1,0:T(1,128)S(1)}, f32[1,512,64]{1,2,0:T(8,128)S(1)}, s32[]{:T(128)}, /*index=5*/s32[512]{...) while((s32[]{:T(128)}, f32[1,512]{1,0:T(1,128)S(1)}, ...), condition=%wide.region_4.4_spmd, body=%wide.region_1.3_spmd.sunk | while | flops 69797376 | bytes 3653843 | solution.py:96
  139.2 0.7 constant_dynamic-slice_fusion.2
  140.9 0.7 constant_dynamic-slice_fusion.2
  142.6 0.7 constant_dynamic-slice_fusion.2
  144.3 0.7 constant_dynamic-slice_fusion.2
  146.0 0.7 constant_dynamic-slice_fusion.2
  147.7 0.7 constant_dynamic-slice_fusion.2
  152.1 0.7 dynamic-slice_bitcast_fusion.5
  154.2 11.9 %while.30 = (s32[]{:T(128)}, f32[1,512]{1,0:T(1,128)S(1)}, f32[1,512]{1,0:T(1,128)S(1)}, f32[1,512,64]{1,2,0:T(8,128)S(1)}, s32[]{:T(128)}, /*index=5*/s32[512]{...) while((s32[]{:T(128)}, f32[1,512]{1,0:T(1,128)S(1)}, ...), condition=%wide.region_4.4_spmd, body=%wide.region_1.3_spmd.sunk | while | flops 69797376 | bytes 3653843 | solution.py:96
  154.3 0.7 constant_dynamic-slice_fusion.2
  156.0 0.7 constant_dynamic-slice_fusion.2
  157.7 0.7 constant_dynamic-slice_fusion.2
  159.4 0.7 constant_dynamic-slice_fusion.2
  161.1 0.7 constant_dynamic-slice_fusion.2
  162.8 0.7 constant_dynamic-slice_fusion.2
  164.5 0.7 constant_dynamic-slice_fusion.2
  168.9 0.7 dynamic-slice_bitcast_fusion.5
  171.0 13.6 %while.30 = (s32[]{:T(128)}, f32[1,512]{1,0:T(1,128)S(1)}, f32[1,512]{1,0:T(1,128)S(1)}, f32[1,512,64]{1,2,0:T(8,128)S(1)}, s32[]{:T(128)}, /*index=5*/s32[512]{...) while((s32[]{:T(128)}, f32[1,512]{1,0:T(1,128)S(1)}, ...), condition=%wide.region_4.4_spmd, body=%wide.region_1.3_spmd.sunk | while | flops 69797376 | bytes 3653843 | solution.py:96
  171.1 0.7 constant_dynamic-slice_fusion.2
  172.8 0.7 constant_dynamic-slice_fusion.2
  174.5 0.7 constant_dynamic-slice_fusion.2
  176.2 0.7 constant_dynamic-slice_fusion.2
  177.9 0.7 constant_dynamic-slice_fusion.2
  179.6 0.7 constant_dynamic-slice_fusion.2
  181.3 0.7 constant_dynamic-slice_fusion.2
  183.0 0.7 constant_dynamic-slice_fusion.2
  184.9 4.0 %all_to_all.25 = bf16[8,2,1,256,64]{3,4,0,2,1:T(8,128)(2,1)S(1)} all-to-all(bf16[8,2,1,256,64]{3,4,0,2,1:T(8,128)(2,1)S(1)} %copy.34), channel_id=1, replica_groups=mesh['sp_0'=8,'sp_1'=2,'dp'=48] {'sp_1'}, dimensions={1} | all-to-all | bytes 1048576 | tf_op jit(solution)/shard_map/all_to_all | solution.py:39
  189.4 20.9 %all_to_all.26 = bf16[8,2,1,256,64]{3,1,4,2,0:T(2,128)(2,1)S(1)} all-to-all(bf16[8,2,1,256,64]{3,1,4,2,0:T(2,128)(2,1)S(1)} %copy.35), channel_id=1, replica_groups=mesh['sp_0'=8,'sp_1'=2,'dp'=48] {'sp_0'}, dimensions={0} | all-to-all | bytes 1048576 | tf_op jit(solution)/shard_map/all_to_all | solution.py:39
  210.4 7.0 %reshape.67 = bf16[2112,1024]{1,0:T(8,128)(2,1)} reshape(bf16[48,44,1024]{2,1,0:T(8,128)(2,1)} %all-gather.3.cloned.1.call-done) | data formatting | bytes 8650752
  217.4 4.5 %fusion.18 = bf16[1,256,2112]{1,2,0:T(8,128)(2,1)} fusion(bf16[2112,1024]{1,0:T(8,128)(2,1)} %reshape.67, bf16[256,1024]{0,1:T(8,128)(2,1)S(1)} %bitcast.105), kind=kOutput, calls=%fused_computation.29 | convolution fusion | flops 1107836928 | bytes 5931008 | tf_op jit(solution)/shard_map/dot_general | solution.py:109
  (337 shorter events, 43.4 us)
Async XLA Ops:
  6.5 4.9 %copy-start = (bf16[1,256,1024]{2,1,0:T(8,128)(2,1)S(1)}, bf16[1,256,1024]{2,1,0:T(8,128)(2,1)}, u32[]{:S(2)}) copy-start(bf16[1,256,1024]{2,1,0:T(8,128)(2,1)} %param.11) | copy-start | bytes 1572868
  19.1 63.1 %all-to-all-start = ((bf16[3,256,1024]{1,0,2:T(4,128)(2,1)}), bf16[3,256,1024]{1,0,2:T(4,128)(2,1)S(1)}, u32[]{:S(2)}, u32[]{:S(2)}) async-start(bf16[3,256,1024]{1,0,2:T(4,128)(2,1)} %pad_maximum_fusion), calls=%async_computation | async-start | bytes 4194304 | tf_op jit(solution)/shard_map/all_to_all | solution.py:13
  33.0 177.4 %all-gather.3.cloned.1.call-start = ((), (), s32[]{:S(2)}) async-start(), calls=%async_computation.3 | async-start | bytes 4816896 | tf_op jit(solution)/shard_map/all_gather | solution.py:108
Sparse Core Ops, SparseCore 0:
  37.5 117.1 all-gather.2
where the time goes:
time: 231 us; the launch traced here: 229 us
  local copies, waits for them, and re-layouts  52.6 us (23%)
  waiting for transfers between devices  49.1 us (21%)
  matrix products  31 us (13%)
  loops' own time  29.7 us (13%)
  blocking collectives  24.8 us (11%)
  starting transfers between devices  14 us (6%)
  other arithmetic  13.9 us (6%)
  between operations  13.6 us (6%)
    all_to_all x1, waiting for transfers between devices, side_by_side(): lax.all_to_all(both, axis, split_axis=split_dim, concat_axis=concat_dim,...  48.4 us
    another operation x1, loops' own time, attend(): outputs = lax.map(one_block, jnp.arange(block_count, dtype=jnp.int32))  27.9 us
    all_to_all x2, blocking collectives, turned_blocks(): lax.all_to_all(pieces, axes[k], split_axis=k, concat_axis=k, tiled=True)  24.8 us
    dynamic_slice x36, local copies, waits for them, and re-layouts, key_step(): lax.dynamic_index_in_dim(gate_blocks, key_block, 0, keepdims=False)  24.7 us
    dot_general x36, matrix products, key_step(): jnp.einsum('qhe,khe->hqk', query_part, key_part, preferred_element_type=j...  15.2 us
    unnamed x9, local copies, waits for them, and re-layouts  14.3 us
    all_to_all x1, starting transfers between devices, side_by_side(): lax.all_to_all(both, axis, split_axis=split_dim, concat_axis=concat_dim,...  14 us
    dot_general x36, matrix products, key_step(): jnp.einsum('hqk,khe->hqe', scores.astype(jnp.bfloat16), value_part, prefe...  11.4 us
  transfers between devices with their start and end apart: 2, of which 1 were waited for; matrix products, arithmetic and copies ran while one was open for 32% of the time, Pallas kernels for 0%

commit v1 on v0

v1 whole, which is shorter than its diff:
```python
import math

import jax
import jax.numpy as jnp
from jax import lax
from jax.experimental import pallas as pl
from jax.experimental.pallas import tpu as pltpu
from jax.sharding import Mesh
from jax.sharding import PartitionSpec as P

SP = ("sp_0", "sp_1")
LOG2E = math.log2(math.e)
VMEM = pl.BlockSpec(memory_space=pltpu.VMEM)
SMEM = pl.BlockSpec(memory_space=pltpu.SMEM)


def swap_halves(a):
    return jnp.concatenate([a[:, 64:], a[:, :64]], axis=1)


def low_lanes(shape):
    return lax.broadcasted_iota(jnp.int32, shape, 1) < 64


def interleave(first, second):
    lanes = low_lanes(first.shape)
    return (
        jnp.where(lanes, first, swap_halves(second)),
        jnp.where(lanes, swap_halves(first), second),
    )


def pack_kernel(queries, keys, values, out):
    for t, ref in enumerate((queries, keys, values)):
        for j in range(out.shape[0] // 2):
            columns = slice(128 * j, 128 * j + 128)
            out[2 * j, t], out[2 * j + 1, t] = interleave(ref[0:128, columns], ref[128:256, columns])


def pack(queries, keys, values):
    rows, width = queries.shape
    heads, steps = width // 64, 4
    return pl.pallas_call(
        pack_kernel,
        grid=(steps,),
        out_shape=jax.ShapeDtypeStruct((heads, 3, rows // 2, 128), jnp.bfloat16),
        in_specs=[pl.BlockSpec((rows, width // steps), lambda i: (0, i))] * 3,
        out_specs=pl.BlockSpec((heads // steps, 3, rows // 2, 128), lambda i: (i, 0, 0, 0)),
        cost_estimate=pl.CostEstimate(flops=1_000_000, bytes_accessed=3_000_000, transcendentals=0),
        compiler_params=pltpu.CompilerParams(vmem_limit_bytes=8 * 2**20),
        name="pack",
    )(queries, keys, values)


def gate_kernel(gate, out):
    row = lax.broadcasted_iota(jnp.int32, (8, 128), 0)
    for n in range(gate.shape[0]):
        g = jnp.broadcast_to(gate[n : n + 1, :] * -LOG2E, (8, 128))
        high = g.astype(jnp.bfloat16).astype(jnp.float32)
        rest = g - high
        middle = rest.astype(jnp.bfloat16).astype(jnp.float32)
        low = rest - middle
        rows = jnp.where(row == 0, high, jnp.where(row == 1, middle, jnp.where(row == 2, low, 0.0)))
        tile = jnp.concatenate(
            [jnp.zeros((64, 128), jnp.float32), rows, jnp.zeros((56, 128), jnp.float32)], axis=0
        )
        out[128 * n : 128 * n + 128, :] = tile.T.astype(jnp.bfloat16)


def gate_columns(gate):
    return pl.pallas_call(
        gate_kernel,
        out_shape=jax.ShapeDtypeStruct((gate.size, 128), jnp.bfloat16),
        in_specs=[VMEM],
        out_specs=VMEM,
        cost_estimate=pl.CostEstimate(flops=10_000_000, bytes_accessed=1_000_000, transcendentals=0),
        compiler_params=pltpu.CompilerParams(vmem_limit_bytes=6 * 2**20),
        name="gate_columns",
    )(gate)


def attend_kernel(parts, gate, out, keys, values, logits):
    count = parts.shape[0]
    lanes = low_lanes((128, 128))
    values[64:80, :] = jnp.ones((16, values.shape[1]), jnp.bfloat16)
    for b in range(count):
        base = 256 * b
        k = parts[b, 1]
        swapped = swap_halves(k)
        keys[base : base + 128, 0:128] = jnp.where(lanes, k, swapped)
        keys[base + 128 : base + 256, 0:128] = jnp.where(lanes, swapped, k)
        keys[base : base + 128, 128:256] = jnp.where(lanes, k, gate[base : base + 128, :])
        keys[base + 128 : base + 256, 128:256] = jnp.where(
            lanes, swapped, gate[base + 128 : base + 256, :]
        )
        v = parts[b, 2].T
        values[0:64, base : base + 128] = v[:64]
        values[0:64, base + 128 : base + 256] = v[64:]
    causal = lax.broadcasted_iota(jnp.int32, (256, 256), 0) <= lax.broadcasted_iota(
        jnp.int32, (256, 256), 1
    )

    def first(i):
        q = parts[i, 0].astype(jnp.float32).T
        q = jnp.concatenate([q[:64], q[64:]], axis=1) * (LOG2E / 8.0)
        high = q.astype(jnp.bfloat16)
        rest = q - high.astype(jnp.float32)
        middle = rest.astype(jnp.bfloat16)
        low = (rest - middle.astype(jnp.float32)).astype(jnp.bfloat16)
        queries = jnp.concatenate([high, middle, low, jnp.ones((64, 256), jnp.bfloat16)], axis=0)
        peak = None
        for j in range(i + 1):
            s = jnp.dot(
                keys[256 * j : 256 * j + 256, :], queries, preferred_element_type=jnp.float32
            )
            if j == i:
                s = jnp.where(causal, s, -jnp.inf)
            logits[i % 2, 256 * j : 256 * j + 256, :] = s
            top = jnp.max(s.reshape(32, 8, 256), axis=0)
            peak = top if peak is None else jnp.maximum(peak, top)
        return jnp.max(peak, axis=0, keepdims=True)

    def second(i, peak):
        total = None
        for j in range(i + 1):
            p = jnp.exp2(logits[i % 2, 256 * j : 256 * j + 256, :] - peak).astype(jnp.bfloat16)
            o = jnp.dot(
                values[:, 256 * j : 256 * j + 256], p, preferred_element_type=jnp.float32
            )
            total = o if total is None else total + o
        out[i] = (total[:64] / total[64:65]).astype(jnp.bfloat16)

    peak = first(0)
    for i in range(count):
        following = first(i + 1) if i + 1 < count else None
        second(i, peak)
        peak = following


def attend(parts, gate):
    count = parts.shape[0]
    length = 256 * count
    return pl.pallas_call(
        attend_kernel,
        out_shape=jax.ShapeDtypeStruct((count, 64, 256), jnp.bfloat16),
        in_specs=[VMEM] * 2,
        out_specs=VMEM,
        scratch_shapes=[
            pltpu.VMEM((length, 256), jnp.bfloat16),
            pltpu.VMEM((80, length), jnp.bfloat16),
            pltpu.VMEM((2, length, 256), jnp.float32),
        ],
        compiler_params=pltpu.CompilerParams(vmem_limit_bytes=32 * 2**20),
        cost_estimate=pl.CostEstimate(
            flops=10_000_000_000, bytes_accessed=4_000_000, transcendentals=9_000_000
        ),
        name="attend",
    )(parts, gate)


def assemble_kernel(me, blocks, out):
    x = me[0]
    hops, groups, columns, _ = blocks.shape
    for k in range(hops):
        hop = lax.rem(x - k + hops, hops)
        for z in range(groups):
            row = columns * (hops * z + k)
            out[row : row + columns, :] = blocks[hop, z]


def assemble(me, blocks):
    hops, groups, columns, depth = blocks.shape
    return pl.pallas_call(
        assemble_kernel,
        out_shape=jax.ShapeDtypeStruct((hops * groups * columns, depth), jnp.bfloat16),
        in_specs=[SMEM, VMEM],
        out_specs=VMEM,
        cost_estimate=pl.CostEstimate(flops=1_000_000, bytes_accessed=4_300_000, transcendentals=0),
        compiler_params=pltpu.CompilerParams(vmem_limit_bytes=16 * 2**20),
        name="assemble",
    )(me, blocks)


def project_kernel(core, attended, mine, other, out):
    heads, depth, rows = attended.shape
    c, half = core[0], heads // 2

    def columns(first):
        return attended[pl.ds(first, half)].reshape(half * depth, rows)

    total = jnp.dot(mine[...], columns(c * half), preferred_element_type=jnp.float32)
    total += jnp.dot(other[...], columns((1 - c) * half), preferred_element_type=jnp.float32)
    out[...] = total.astype(jnp.bfloat16)


def project(core, attended, mine, other):
    columns = mine.shape[0]
    return pl.pallas_call(
        project_kernel,
        out_shape=jax.ShapeDtypeStruct((columns, attended.shape[2]), jnp.bfloat16),
        in_specs=[SMEM] + [VMEM] * 3,
        out_specs=VMEM,
        compiler_params=pltpu.CompilerParams(vmem_limit_bytes=16 * 2**20),
        cost_estimate=pl.CostEstimate(
            flops=1_100_000_000, bytes_accessed=6_000_000, transcendentals=0
        ),
        name="project",
    )(core, attended, mine, other)


def body(queries, keys, values, cum_gate, out_weight):
    core, x = lax.axis_index("sp_1"), lax.axis_index("x")
    packed = pack(queries[0], keys[0], values[0])
    parts = lax.all_to_all(packed, SP, 0, 0, tiled=True)
    gate = gate_columns(cum_gate[0, 0].reshape(-1, 128))

    depth = out_weight.shape[0] // 2
    own = lax.dynamic_slice_in_dim(out_weight.T, core * depth, depth, axis=1)
    along_z = lax.all_gather(own[None], "z", axis=0, tiled=True)
    n = lax.axis_size("x")
    blocks = [along_z] + [
        lax.ppermute(along_z, "x", [(i, (i + hop) % n) for i in range(n)]) for hop in range(1, n)
    ]
    mine = assemble(x.reshape(1), jnp.stack(blocks))
    other = lax.ppermute(mine, "sp_1", [(0, 1), (1, 0)])

    local = attend(parts, gate)
    back = lax.all_to_all(local, SP, 0, 0, tiled=True)
    return project(core.reshape(1), back, mine, other).T[None]


def solution(mesh):
    split = Mesh(mesh.devices.reshape(8, 2, 12, 4), ("sp_0", "sp_1", "z", "x"))
    dp = ("z", "x")
    return jax.shard_map(
        body,
        mesh=split,
        in_specs=(P(dp, SP, None), P(dp, SP, None), P(dp, SP, None), P(dp, SP, None), P(None, dp)),
        out_specs=P(dp, SP, None),
        check_vma=False,
    )
```

time: 231 us -> 127 us (0.55)
  local copies, waits for them, and re-layouts: 52.6 us -> 3.97 us
  matrix products: 31 us -> 0 us
  loops' own time: 29.7 us -> 0 us
  starting transfers between devices: 14 us -> 33.5 us
  Pallas kernels: 0 us -> 19.3 us
  other arithmetic: 13.9 us -> 0.31 us
  between operations: 13.6 us -> 0.11 us
  waiting for transfers between devices: 49.1 us -> 43.5 us
    all_to_all x1 -> x2, waiting for transfers between devices: 48.4 us -> 17.2 us  [the longest x1 17.2 us: body(): back = lax.all_to_all(local, SP, 0, 0, tiled=True)]
    dot_general x73 -> x0, matrix products: 31 us -> none  [the longest x36 15.2 us: key_step(): jnp.einsum('qhe,khe->hqk', query_part, key_part, preferred_element_type=j...]
    dynamic_slice x44 -> x0, local copies, waits for them, and re-layouts: 30 us -> none  [the longest x36 24.7 us: key_step(): lax.dynamic_index_in_dim(gate_blocks, key_block, 0, keepdims=False)]
    another operation x9 -> x0, loops' own time: 29.7 us -> none  [the longest x1 27.9 us: attend(): outputs = lax.map(one_block, jnp.arange(block_count, dtype=jnp.int32))]
    ppermute x0 -> x4, waiting for transfers between devices: none -> 26.3 us  [the longest x3 26.3 us: body(): lax.ppermute(along_z, 'x', [(i, (i + hop) % n) for i in range(n)])]
    all_gather x0 -> x1, blocking collectives: none -> 25.9 us  [body(): along_z = lax.all_gather(own[None], 'z', axis=0, tiled=True)]
    all_to_all x2 -> x0, blocking collectives: 24.8 us -> none  [turned_blocks(): lax.all_to_all(pieces, axes[k], split_axis=k, concat_axis=k, tiled=True)]
    pallas_call x0 -> x5, Pallas kernels: none -> 19.3 us  [the longest x1 12.6 us: attend(): pl.pallas_call(attend_kernel, out_shape=jax.ShapeDtypeStruct((count, 64,...]
  transfers between devices with their start and end apart: 2 -> 6, of which waited for: 1 -> 4; matrix products, arithmetic and copies ran while one was open for 32% -> 0% of each run, Pallas kernels for 0% -> 10%
where the time goes in v1:
time: 127 us
  waiting for transfers between devices  43.5 us (34%)
  starting transfers between devices  33.5 us (26%)
  blocking collectives  25.9 us (20%)
  Pallas kernels  19.3 us (15%)
  local copies, waits for them, and re-layouts  3.97 us (3%)
    ppermute x3, waiting for transfers between devices, body(): lax.ppermute(along_z, 'x', [(i, (i + hop) % n) for i in range(n)])  26.3 us
    all_gather x1, blocking collectives, body(): along_z = lax.all_gather(own[None], 'z', axis=0, tiled=True)  25.9 us
    all_to_all x1, waiting for transfers between devices, body(): back = lax.all_to_all(local, SP, 0, 0, tiled=True)  17.2 us
    all_to_all x1, starting transfers between devices, body(): parts = lax.all_to_all(packed, SP, 0, 0, tiled=True)  14.6 us
    pallas_call x1, Pallas kernels, attend(): pl.pallas_call(attend_kernel, out_shape=jax.ShapeDtypeStruct((count, 64,...  12.6 us
    ppermute x3, starting transfers between devices, body(): lax.ppermute(along_z, 'x', [(i, (i + hop) % n) for i in range(n)])  9.16 us
    all_to_all x1, starting transfers between devices, body(): back = lax.all_to_all(local, SP, 0, 0, tiled=True)  7.33 us
    unnamed x13, local copies, waits for them, and re-layouts  3.97 us
  transfers between devices with their start and end apart: 6, of which 4 were waited for; matrix products, arithmetic and copies ran while one was open for 0% of the time, Pallas kernels for 10%

profile of v1, /device:TPU:1, one launch (start us, length us, event | category | flops | bytes accessed | tf_op | source)
XLA Modules:
  0.0 126.6 jit_solution(15033757783635792558)
XLA Ops:
  0.0 0.0 copy-start
  0.0 0.0 copy-start.2
  0.0 1.1 copy-done.2
  1.1 0.0 copy-start.3
  1.1 1.0 copy-done.3
  2.1 0.0 copy-start.4
  2.1 1.0 copy-done.4
  3.2 2.2 %pack.1 = bf16[16,3,128,128]{3,2,1,0:T(8,128)(2,1)} custom-call(bf16[256,1024]{1,0:T(8,128)(2,1)S(1)} %bitcast.17, bf16[256,1024]{1,0:T(8,128)(2,1)S(1)} %bitcast.18, bf16[256,1024]{1,0:T(8,128)(2,1)S(1)} %bitcast.19), custom_call_target="tpu_custom_call" | custom-call | flops 1000000 | bytes 3000000 | tf_op jit(solution)/shard_map/pack/pallas_call | solution.py:43
  5.4 14.6 %all-to-all-start = ((bf16[16,3,128,128]{3,2,1,0:T(8,128)(2,1)}), bf16[16,3,128,128]{3,2,1,0:T(8,128)(2,1)}, u32[]{:S(2)}, u32[]{:S(2)}) async-start(bf16[16,3,128,128]{3,2,1,0:T(8,128)(2,1)} %pack.1), calls=%async_computation | async-start | bytes 3145728 | tf_op jit(solution)/shard_map/all_to_all | solution.py:214
  20.0 0.0 copy-done
  20.0 25.9 %all-gather.1 = bf16[12,44,512]{2,1,0:T(8,128)(2,1)S(1)} all-gather(bf16[1,44,512]{2,1,0:T(8,128)(2,1)S(1)} %dynamic-slice_bitcast_fusion), channel_id=2, replica_groups=mesh['sp_0'=8,'sp_1'=2,'z'=12,'x'=4] {'z'}, dimensions={0}, use_global_device_ids=true | all-gather | bytes 585728 | tf_op jit(solution)/shard_map/all_gather | solution.py:219
  45.9 4.2 %collective-permute-start.2 = (bf16[12,44,512]{2,1,0:T(8,128)(2,1)S(1)}, bf16[12,44,512]{2,1,0:T(8,128)(2,1)S(1)}, u32[]{:S(2)}, u32[]{:S(2)}) collective-permute-start(bf16[12,44,512]{2,1,0:T(8,128)(2,1)S(1)} %all-gather.1), channel_id=1, source_target_pairs={{0,3},{1,0},{2,1},{3,2},{4,7},{5,4},{6,5},{7,6},{8,11},{9,8},{10,9... | collective-permute-start | bytes 1622024 | tf_op jit(solution)/shard_map/ppermute | solution.py:222
  50.2 2.4 %collective-permute-start.1 = (bf16[12,44,512]{2,1,0:T(8,128)(2,1)S(1)}, bf16[12,44,512]{2,1,0:T(8,128)(2,1)S(1)}, u32[]{:S(2)}, u32[]{:S(2)}) collective-permute-start(bf16[12,44,512]{2,1,0:T(8,128)(2,1)S(1)} %all-gather.1), channel_id=1, source_target_pairs={{0,2},{1,3},{2,0},{3,1},{4,6},{5,7},{6,4},{7,5},{8,10},{9,11},{10,... | collective-permute-start | bytes 1622024 | tf_op jit(solution)/shard_map/ppermute | solution.py:222
  52.6 2.5 %collective-permute-start = (bf16[12,44,512]{2,1,0:T(8,128)(2,1)S(1)}, bf16[12,44,512]{2,1,0:T(8,128)(2,1)S(1)}, u32[]{:S(2)}, u32[]{:S(2)}) collective-permute-start(bf16[12,44,512]{2,1,0:T(8,128)(2,1)S(1)} %all-gather.1), channel_id=1, source_target_pairs={{0,1},{1,2},{2,3},{3,0},{4,5},{5,6},{6,7},{7,4},{8,9},{9,10},{10,1... | collective-permute-start | bytes 1622024 | tf_op jit(solution)/shard_map/ppermute | solution.py:222
  55.1 4.0 %collective-permute-done.2 = bf16[12,44,512]{2,1,0:T(8,128)(2,1)S(1)} collective-permute-done((bf16[12,44,512]{2,1,0:T(8,128)(2,1)S(1)}, bf16[12,44,512]{2,1,0:T(8,128)(2,1)S(1)}, u32[]{:S(2)}, u32[]{:S(2)}) %collective-permute-start.2) | collective-permute-done | bytes 540704 | tf_op jit(solution)/shard_map/ppermute | solution.py:222
  59.1 5.0 %collective-permute-done.1 = bf16[12,44,512]{2,1,0:T(8,128)(2,1)S(1)} collective-permute-done((bf16[12,44,512]{2,1,0:T(8,128)(2,1)S(1)}, bf16[12,44,512]{2,1,0:T(8,128)(2,1)S(1)}, u32[]{:S(2)}, u32[]{:S(2)}) %collective-permute-start.1) | collective-permute-done | bytes 540704 | tf_op jit(solution)/shard_map/ppermute | solution.py:222
  64.0 17.4 %collective-permute-done = bf16[12,44,512]{2,1,0:T(8,128)(2,1)S(1)} collective-permute-done((bf16[12,44,512]{2,1,0:T(8,128)(2,1)S(1)}, bf16[12,44,512]{2,1,0:T(8,128)(2,1)S(1)}, u32[]{:S(2)}, u32[]{:S(2)}) %collective-permute-start) | collective-permute-done | bytes 540704 | tf_op jit(solution)/shard_map/ppermute | solution.py:222
  81.5 0.3 pad_maximum_fusion.blocks
  81.8 0.0 copy-start.5
  81.8 0.2 assemble.1.mine
  82.0 2.4 %collective-permute-start.3 = (bf16[2112,512]{1,0:T(8,128)(2,1)S(1)}, bf16[2112,512]{1,0:T(8,128)(2,1)}, u32[]{:S(2)}, u32[]{:S(2)}) collective-permute-start(bf16[2112,512]{1,0:T(8,128)(2,1)S(1)} %assemble.1.mine), channel_id=1, source_target_pairs={{0,48},{48,0},{1,49},{49,1},{2,50},{50,2},{3,51},{51,3},{4,52},{52... | collective-permute-start | bytes 6488072 | tf_op jit(solution)/shard_map/ppermute | solution.py:225
  84.4 0.0 copy-done.5
  84.4 0.3 gate_columns.1.gate
  84.8 0.0 all-to-all-done.parts
  84.8 12.6 %attend.1 = bf16[16,64,256]{2,1,0:T(8,128)(2,1)S(1)} custom-call(bf16[16,3,128,128]{3,2,1,0:T(8,128)(2,1)} %all-to-all-done.parts, bf16[4096,128]{1,0:T(8,128)(2,1)S(1)} %gate_columns.1.gate), custom_call_target="tpu_custom_call" | custom-call | flops 10000000000 | bytes 4000000 | tf_op jit(solution)/shard_map/attend/pallas_call | solution.py:143
  97.4 0.0 copy-start.1
  97.4 0.8 copy-done.1
  98.2 7.3 %all-to-all-start.1 = ((bf16[16,64,256]{2,1,0:T(8,128)(2,1)}), bf16[16,64,256]{2,1,0:T(8,128)(2,1)S(1)}, u32[]{:S(2)}, u32[]{:S(2)}) async-start(bf16[16,64,256]{2,1,0:T(8,128)(2,1)} %copy-done.1), calls=%async_computation.1 | async-start | bytes 1048576 | tf_op jit(solution)/shard_map/all_to_all | solution.py:228
  105.5 0.0 collective-permute-done.3.other
  105.5 17.2 %all-to-all-done.1.attended = bf16[16,64,256]{2,1,0:T(8,128)(2,1)S(1)} async-done(((bf16[16,64,256]{2,1,0:T(8,128)(2,1)}), bf16[16,64,256]{2,1,0:T(8,128)(2,1)S(1)}, u32[]{:S(2)}, u32[]{:S(2)}) %all-to-all-start.1) | async-done | bytes 524320 | tf_op jit(solution)/shard_map/all_to_all | solution.py:228
  122.7 3.9 %project.1 = bf16[2112,256]{1,0:T(8,128)(2,1)} custom-call(s32[1]{0:T(128)} %bitcast.core, bf16[16,64,256]{2,1,0:T(8,128)(2,1)S(1)} %all-to-all-done.1.attended, bf16[2112,512]{1,0:T(8,128)(2,1)S(1)} %assemble.1.mine, bf16[2112,512]{1,0:T(8,128)(2,1)} %collective-permute-done.3.other), custom_call_target="tpu_custom_call" | custom-call | flops 1100000000 | bytes 6000000 | tf_op jit(solution)/shard_map/project/pallas_call | solution.py:198
  (1 shorter events, 0.0 us)
Async XLA Ops:
  0.0 20.0 %copy-start = (bf16[1024,44]{0,1:T(8,128)(2,1)S(1)}, bf16[1024,44]{0,1:T(8,128)(2,1)}, u32[]{:S(2)}) copy-start(bf16[1024,44]{0,1:T(8,128)(2,1)} %param.9) | copy-start | bytes 270340
  0.0 1.1 copy-start.2
  1.1 1.0 copy-start.3
  2.1 1.0 copy-start.4
  5.4 79.4 %all-to-all-start = ((bf16[16,3,128,128]{3,2,1,0:T(8,128)(2,1)}), bf16[16,3,128,128]{3,2,1,0:T(8,128)(2,1)}, u32[]{:S(2)}, u32[]{:S(2)}) async-start(bf16[16,3,128,128]{3,2,1,0:T(8,128)(2,1)} %pack.1), calls=%async_computation | async-start | bytes 3145728 | tf_op jit(solution)/shard_map/all_to_all | solution.py:214
  45.9 13.2 %collective-permute-start.2 = (bf16[12,44,512]{2,1,0:T(8,128)(2,1)S(1)}, bf16[12,44,512]{2,1,0:T(8,128)(2,1)S(1)}, u32[]{:S(2)}, u32[]{:S(2)}) collective-permute-start(bf16[12,44,512]{2,1,0:T(8,128)(2,1)S(1)} %all-gather.1), channel_id=1, source_target_pairs={{0,3},{1,0},{2,1},{3,2},{4,7},{5,4},{6,5},{7,6},{8,11},{9,8},{10,9... | collective-permute-start | bytes 1622024 | tf_op jit(solution)/shard_map/ppermute | solution.py:222
  50.2 13.9 %collective-permute-start.1 = (bf16[12,44,512]{2,1,0:T(8,128)(2,1)S(1)}, bf16[12,44,512]{2,1,0:T(8,128)(2,1)S(1)}, u32[]{:S(2)}, u32[]{:S(2)}) collective-permute-start(bf16[12,44,512]{2,1,0:T(8,128)(2,1)S(1)} %all-gather.1), channel_id=1, source_target_pairs={{0,2},{1,3},{2,0},{3,1},{4,6},{5,7},{6,4},{7,5},{8,10},{9,11},{10,... | collective-permute-start | bytes 1622024 | tf_op jit(solution)/shard_map/ppermute | solution.py:222
  52.6 28.9 %collective-permute-start = (bf16[12,44,512]{2,1,0:T(8,128)(2,1)S(1)}, bf16[12,44,512]{2,1,0:T(8,128)(2,1)S(1)}, u32[]{:S(2)}, u32[]{:S(2)}) collective-permute-start(bf16[12,44,512]{2,1,0:T(8,128)(2,1)S(1)} %all-gather.1), channel_id=1, source_target_pairs={{0,1},{1,2},{2,3},{3,0},{4,5},{5,6},{6,7},{7,4},{8,9},{9,10},{10,1... | collective-permute-start | bytes 1622024 | tf_op jit(solution)/shard_map/ppermute | solution.py:222
  81.8 2.6 %copy-start.5 = (f32[1,1,4096]{2,1,0:T(1,128)S(1)}, f32[1,1,4096]{2,1,0:T(1,128)}, u32[]{:S(2)}) copy-start(f32[1,1,4096]{2,1,0:T(1,128)} %param.8) | copy-start | bytes 49156
  82.0 23.6 %collective-permute-start.3 = (bf16[2112,512]{1,0:T(8,128)(2,1)S(1)}, bf16[2112,512]{1,0:T(8,128)(2,1)}, u32[]{:S(2)}, u32[]{:S(2)}) collective-permute-start(bf16[2112,512]{1,0:T(8,128)(2,1)S(1)} %assemble.1.mine), channel_id=1, source_target_pairs={{0,48},{48,0},{1,49},{49,1},{2,50},{50,2},{3,51},{51,3},{4,52},{52... | collective-permute-start | bytes 6488072 | tf_op jit(solution)/shard_map/ppermute | solution.py:225
  97.4 0.8 copy-start.1
  98.2 24.5 %all-to-all-start.1 = ((bf16[16,64,256]{2,1,0:T(8,128)(2,1)}), bf16[16,64,256]{2,1,0:T(8,128)(2,1)S(1)}, u32[]{:S(2)}, u32[]{:S(2)}) async-start(bf16[16,64,256]{2,1,0:T(8,128)(2,1)} %copy-done.1), calls=%async_computation.1 | async-start | bytes 1048576 | tf_op jit(solution)/shard_map/all_to_all | solution.py:228

commit v2 on v1

--- a/solution.py
+++ b/solution.py
@@ -8,10 +8,12 @@
 from jax.sharding import Mesh
 from jax.sharding import PartitionSpec as P
 
+
 SP = ("sp_0", "sp_1")
 LOG2E = math.log2(math.e)
 VMEM = pl.BlockSpec(memory_space=pltpu.VMEM)
 SMEM = pl.BlockSpec(memory_space=pltpu.SMEM)
+HBM = pl.BlockSpec(memory_space=pltpu.HBM)
 
 
 def swap_halves(a):
@@ -30,24 +32,54 @@
     )
 
 
-def pack_kernel(queries, keys, values, out):
-    for t, ref in enumerate((queries, keys, values)):
-        for j in range(out.shape[0] // 2):
-            columns = slice(128 * j, 128 * j + 128)
-            out[2 * j, t], out[2 * j + 1, t] = interleave(ref[0:128, columns], ref[128:256, columns])
+def pack_kernel(queries, keys, values, out, taken, packed, arrived, left):
+    heads = out.shape[0]
+    groups = arrived.shape[0]
+    width, each = taken.shape[2] // groups, heads // groups
+
+    def arrival(g, t):
+        columns = slice(width * g, width * g + width)
+        source = (queries, keys, values)[t]
+        return pltpu.make_async_copy(
+            source.at[:, columns], taken.at[t, :, columns], arrived.at[g, t]
+        )
+
+    def departure(g):
+        block = slice(each * g, each * g + each)
+        return pltpu.make_async_copy(packed.at[block], out.at[block], left.at[g])
+
+    for g in range(groups):
+        for t in range(3):
+            arrival(g, t).start()
+    for g in range(groups):
+        for t in range(3):
+            arrival(g, t).wait()
+            for j in range(each * g // 2, (each * g + each) // 2):
+                columns = slice(128 * j, 128 * j + 128)
+                packed[2 * j, t], packed[2 * j + 1, t] = interleave(
+                    taken[t, 0:128, columns], taken[t, 128:256, columns]
+                )
+        departure(g).start()
+    for g in range(groups):
+        departure(g).wait()
 
 
 def pack(queries, keys, values):
     rows, width = queries.shape
-    heads, steps = width // 64, 4
+    heads, groups = width // 64, 4
     return pl.pallas_call(
         pack_kernel,
-        grid=(steps,),
         out_shape=jax.ShapeDtypeStruct((heads, 3, rows // 2, 128), jnp.bfloat16),
-        in_specs=[pl.BlockSpec((rows, width // steps), lambda i: (0, i))] * 3,
-        out_specs=pl.BlockSpec((heads // steps, 3, rows // 2, 128), lambda i: (i, 0, 0, 0)),
+        in_specs=[HBM] * 3,
+        out_specs=HBM,
+        scratch_shapes=[
+            pltpu.VMEM((3, rows, width), jnp.bfloat16),
+            pltpu.VMEM((heads, 3, rows // 2, 128), jnp.bfloat16),
+            pltpu.SemaphoreType.DMA((groups, 3)),
+            pltpu.SemaphoreType.DMA((groups,)),
+        ],
+        compiler_params=pltpu.CompilerParams(vmem_limit_bytes=60 * 2**20),
         cost_estimate=pl.CostEstimate(flops=1_000_000, bytes_accessed=3_000_000, transcendentals=0),
-        compiler_params=pltpu.CompilerParams(vmem_limit_bytes=8 * 2**20),
         name="pack",
     )(queries, keys, values)
 
@@ -79,12 +111,28 @@
     )(gate)
 
 
-def attend_kernel(parts, gate, out, keys, values, logits):
+def attend_kernel(source, columns, out, parts, gate, keys, values, logits, finished, arrived, left):
     count = parts.shape[0]
+
+    def arrival(b):
+        rows = slice(256 * b, 256 * b + 256)
+        return (
+            pltpu.make_async_copy(source.at[b], parts.at[b], arrived.at[b, 0]),
+            pltpu.make_async_copy(columns.at[rows], gate.at[rows], arrived.at[b, 1]),
+        )
+
+    def departure(b):
+        return pltpu.make_async_copy(finished.at[b], out.at[b], left.at[b])
+
+    for b in range(count):
+        for copy in arrival(b):
+            copy.start()
     lanes = low_lanes((128, 128))
     values[64:80, :] = jnp.ones((16, values.shape[1]), jnp.bfloat16)
     for b in range(count):
         base = 256 * b
+        for copy in arrival(b):
+            copy.wait()
         k = parts[b, 1]
         swapped = swap_halves(k)
         keys[base : base + 128, 0:128] = jnp.where(lanes, k, swapped)
@@ -128,13 +176,16 @@
                 values[:, 256 * j : 256 * j + 256], p, preferred_element_type=jnp.float32
             )
             total = o if total is None else total + o
-        out[i] = (total[:64] / total[64:65]).astype(jnp.bfloat16)
+        finished[i] = (total[:64] / total[64:65]).astype(jnp.bfloat16)
+        departure(i).start()
 
     peak = first(0)
     for i in range(count):
         following = first(i + 1) if i + 1 < count else None
         second(i, peak)
         peak = following
+    for i in range(count):
+        departure(i).wait()
 
 
 def attend(parts, gate):
@@ -143,14 +194,19 @@
     return pl.pallas_call(
         attend_kernel,
         out_shape=jax.ShapeDtypeStruct((count, 64, 256), jnp.bfloat16),
-        in_specs=[VMEM] * 2,
-        out_specs=VMEM,
+        in_specs=[HBM, HBM],
+        out_specs=HBM,
         scratch_shapes=[
+            pltpu.VMEM(parts.shape, jnp.bfloat16),
+            pltpu.VMEM(gate.shape, jnp.bfloat16),
             pltpu.VMEM((length, 256), jnp.bfloat16),
             pltpu.VMEM((80, length), jnp.bfloat16),
             pltpu.VMEM((2, length, 256), jnp.float32),
+            pltpu.VMEM((count, 64, 256), jnp.bfloat16),
+            pltpu.SemaphoreType.DMA((count, 2)),
+            pltpu.SemaphoreType.DMA((count,)),
         ],
-        compiler_params=pltpu.CompilerParams(vmem_limit_bytes=32 * 2**20),
+        compiler_params=pltpu.CompilerParams(vmem_limit_bytes=60 * 2**20),
         cost_estimate=pl.CostEstimate(
             flops=10_000_000_000, bytes_accessed=4_000_000, transcendentals=9_000_000
         ),
@@ -158,27 +214,34 @@
     )(parts, gate)
 
 
-def assemble_kernel(me, blocks, out):
-    x = me[0]
-    hops, groups, columns, _ = blocks.shape
+def assemble_kernel(me, after, *refs):
+    del after
+    *blocks, out = refs
+    hops = len(blocks)
+    groups, columns, _ = blocks[0].shape
     for k in range(hops):
-        hop = lax.rem(x - k + hops, hops)
-        for z in range(groups):
-            row = columns * (hops * z + k)
-            out[row : row + columns, :] = blocks[hop, z]
-
-
-def assemble(me, blocks):
-    hops, groups, columns, depth = blocks.shape
+        for hop in range(hops):
+
+            @pl.when(lax.rem(me[0] - k + hops, hops) == hop)
+            def _():
+                @pl.loop(0, groups)
+                def _(z):
+                    first = pl.multiple_of(hops * columns * z, 8)
+                    group = out.at[pl.ds(first, hops * columns)]
+                    group[columns * k : columns * k + columns, :] = blocks[hop][z]
+
+
+def assemble(me, after, blocks):
+    groups, columns, depth = blocks[0].shape
     return pl.pallas_call(
         assemble_kernel,
-        out_shape=jax.ShapeDtypeStruct((hops * groups * columns, depth), jnp.bfloat16),
-        in_specs=[SMEM, VMEM],
+        out_shape=jax.ShapeDtypeStruct((len(blocks) * groups * columns, depth), jnp.bfloat16),
+        in_specs=[SMEM, pl.BlockSpec(memory_space=pl.ANY)] + [VMEM] * len(blocks),
         out_specs=VMEM,
+        compiler_params=pltpu.CompilerParams(vmem_limit_bytes=60 * 2**20),
         cost_estimate=pl.CostEstimate(flops=1_000_000, bytes_accessed=4_300_000, transcendentals=0),
-        compiler_params=pltpu.CompilerParams(vmem_limit_bytes=16 * 2**20),
         name="assemble",
-    )(me, blocks)
+    )(me, after, *blocks)
 
 
 def project_kernel(core, attended, mine, other, out):
@@ -194,12 +257,18 @@
 
 
 def project(core, attended, mine, other):
-    columns = mine.shape[0]
+    columns, step = mine.shape[0], 352
     return pl.pallas_call(
         project_kernel,
         out_shape=jax.ShapeDtypeStruct((columns, attended.shape[2]), jnp.bfloat16),
-        in_specs=[SMEM] + [VMEM] * 3,
-        out_specs=VMEM,
+        grid=(columns // step,),
+        in_specs=[
+            SMEM,
+            pl.BlockSpec(attended.shape, lambda i: (0, 0, 0)),
+            pl.BlockSpec((step, mine.shape[1]), lambda i: (i, 0)),
+            pl.BlockSpec((step, other.shape[1]), lambda i: (i, 0)),
+        ],
+        out_specs=pl.BlockSpec((step, attended.shape[2]), lambda i: (i, 0)),
         compiler_params=pltpu.CompilerParams(vmem_limit_bytes=16 * 2**20),
         cost_estimate=pl.CostEstimate(
             flops=1_100_000_000, bytes_accessed=6_000_000, transcendentals=0
@@ -219,12 +288,12 @@
     along_z = lax.all_gather(own[None], "z", axis=0, tiled=True)
     n = lax.axis_size("x")
     blocks = [along_z] + [
-        lax.ppermute(along_z, "x", [(i, (i + hop) % n) for i in range(n)]) for hop in range(1, n)
+        lax.ppermute(along_z, "x", [(i, (i + hop) % n) for i in range(n)])
+        for hop in range(1, n)
     ]
-    mine = assemble(x.reshape(1), jnp.stack(blocks))
+    local = attend(parts, gate)
+    mine = assemble(x.reshape(1), local, blocks)
     other = lax.ppermute(mine, "sp_1", [(0, 1), (1, 0)])
-
-    local = attend(parts, gate)
     back = lax.all_to_all(local, SP, 0, 0, tiled=True)
     return project(core.reshape(1), back, mine, other).T[None]
 

time: 127 us -> 113 us (0.89)
  waiting for transfers between devices: 43.5 us -> 4.26 us
  blocking collectives: 25.9 us -> 50.3 us
  Pallas kernels: 19.3 us -> 24.6 us
  starting transfers between devices: 33.5 us -> 29 us
    all_to_all x0 -> x1, blocking collectives: none -> 24.2 us  [body(): back = lax.all_to_all(local, SP, 0, 0, tiled=True)]
    ppermute x3, waiting for transfers between devices: 26.3 us -> 3.62 us  [body(): lax.ppermute(along_z, 'x', [(i, (i + hop) % n) for i in range(n)])]
    all_to_all x1 -> x0, waiting for transfers between devices: 17.2 us -> none  [body(): back = lax.all_to_all(local, SP, 0, 0, tiled=True)]
    all_to_all x1 -> x0, starting transfers between devices: 7.33 us -> none  [body(): back = lax.all_to_all(local, SP, 0, 0, tiled=True)]
    pallas_call x2, Pallas kernels: 2.43 us -> 6.67 us  [the longest x1 3.56 us: assemble(): pl.pallas_call(assemble_kernel, out_shape=jax.ShapeDtypeStruct((len(block...]
    ppermute x1, starting transfers between devices: 2.4 us -> 4.53 us  [body(): other = lax.ppermute(mine, 'sp_1', [(0, 1), (1, 0)])]
    pallas_call x1, Pallas kernels: 12.6 us -> 14.1 us  [attend(): pl.pallas_call(attend_kernel, out_shape=jax.ShapeDtypeStruct((count, 64,...]
    ppermute x3, starting transfers between devices: 9.16 us -> 10.5 us  [body(): lax.ppermute(along_z, 'x', [(i, (i + hop) % n) for i in range(n)])]
  transfers between devices with their start and end apart: 6 -> 5, of which waited for: 4 -> 2; matrix products, arithmetic and copies ran while one was open for 0% -> 0% of each run, Pallas kernels for 10% -> 13%
where the time goes in v2:
time: 113 us; the launch traced here: 112 us
  blocking collectives  50.3 us (45%)
  starting transfers between devices  29 us (26%)
  Pallas kernels  24.6 us (22%)
  waiting for transfers between devices  4.26 us (4%)
  local copies, waits for them, and re-layouts  3.78 us (3%)
    all_gather x1, blocking collectives, body(): along_z = lax.all_gather(own[None], 'z', axis=0, tiled=True)  26 us
    all_to_all x1, blocking collectives, body(): back = lax.all_to_all(local, SP, 0, 0, tiled=True)  24.2 us
    pallas_call x1, Pallas kernels, attend(): pl.pallas_call(attend_kernel, out_shape=jax.ShapeDtypeStruct((count, 64,...  14.1 us
    all_to_all x1, starting transfers between devices, body(): parts = lax.all_to_all(packed, SP, 0, 0, tiled=True)  14 us
    ppermute x3, starting transfers between devices, body(): lax.ppermute(along_z, 'x', [(i, (i + hop) % n) for i in range(n)])  10.5 us
    ppermute x1, starting transfers between devices, body(): other = lax.ppermute(mine, 'sp_1', [(0, 1), (1, 0)])  4.53 us
    unnamed x19, local copies, waits for them, and re-layouts  3.78 us
    ppermute x3, waiting for transfers between devices, body(): lax.ppermute(along_z, 'x', [(i, (i + hop) % n) for i in range(n)])  3.62 us
  transfers between devices with their start and end apart: 5, of which 2 were waited for; matrix products, arithmetic and copies ran while one was open for 0% of the time, Pallas kernels for 13%

profile of v2, /device:TPU:1, one launch (start us, length us, event | category | flops | bytes accessed | tf_op | source)
XLA Modules:
  0.0 112.1 jit_solution(4925387406405508798)
XLA Ops:
  0.0 0.0 copy-start
  0.0 3.1 %pack.1 = bf16[16,3,128,128]{3,2,1,0:T(8,128)(2,1)} custom-call(bf16[256,1024]{1,0:T(8,128)(2,1)} %bitcast.14, bf16[256,1024]{1,0:T(8,128)(2,1)} %bitcast.15, bf16[256,1024]{1,0:T(8,128)(2,1)} %bitcast.16), custom_call_target="tpu_custom_call" | custom-call | flops 1000000 | bytes 3000000 | tf_op jit(solution)/shard_map/pack/pallas_call | solution.py:70
  3.1 0.0 copy-start.3
  3.1 14.0 %all-to-all-start = ((bf16[16,3,128,128]{3,2,1,0:T(8,128)(2,1)}), bf16[16,3,128,128]{3,2,1,0:T(8,128)(2,1)S(1)}, u32[]{:S(2)}, u32[]{:S(2)}) async-start(bf16[16,3,128,128]{3,2,1,0:T(8,128)(2,1)} %pack.1), calls=%async_computation | async-start | bytes 3145728 | tf_op jit(solution)/shard_map/all_to_all | solution.py:283
  17.1 0.0 copy-done
  17.1 26.0 %all-gather.1.refs_0_ = bf16[12,44,512]{2,1,0:T(8,128)(2,1)S(1)} all-gather(bf16[1,44,512]{2,1,0:T(8,128)(2,1)S(1)} %dynamic-slice_bitcast_fusion), channel_id=2, replica_groups=mesh['sp_0'=8,'sp_1'=2,'z'=12,'x'=4] {'z'}, dimensions={0}, use_global_device_ids=true | all-gather | bytes 585728 | tf_op jit(solution)/shard_map/all_gather | solution.py:288
  43.2 0.0 copy-start.4
  43.2 3.1 %collective-permute-start = (bf16[12,44,512]{2,1,0:T(8,128)(2,1)S(1)}, bf16[12,44,512]{2,1,0:T(8,128)(2,1)S(1)}, u32[]{:S(2)}, u32[]{:S(2)}) collective-permute-start(bf16[12,44,512]{2,1,0:T(8,128)(2,1)S(1)} %all-gather.1.refs_0_), channel_id=1, source_target_pairs={{0,1},{1,2},{2,3},{3,0},{4,5},{5,6},{6,7},{7,4},{8,9},{9,10},{10,1... | collective-permute-start | bytes 1622024 | tf_op jit(solution)/shard_map/ppermute | solution.py:291
  46.3 4.4 %collective-permute-start.1 = (bf16[12,44,512]{2,1,0:T(8,128)(2,1)S(1)}, bf16[12,44,512]{2,1,0:T(8,128)(2,1)S(1)}, u32[]{:S(2)}, u32[]{:S(2)}) collective-permute-start(bf16[12,44,512]{2,1,0:T(8,128)(2,1)S(1)} %all-gather.1.refs_0_), channel_id=1, source_target_pairs={{0,2},{1,3},{2,0},{3,1},{4,6},{5,7},{6,4},{7,5},{8,10},{9,11},{10,... | collective-permute-start | bytes 1622024 | tf_op jit(solution)/shard_map/ppermute | solution.py:291
  50.7 3.1 %collective-permute-start.2 = (bf16[12,44,512]{2,1,0:T(8,128)(2,1)S(1)}, bf16[12,44,512]{2,1,0:T(8,128)(2,1)}, u32[]{:S(2)}, u32[]{:S(2)}) collective-permute-start(bf16[12,44,512]{2,1,0:T(8,128)(2,1)S(1)} %all-gather.1.refs_0_), channel_id=1, source_target_pairs={{0,3},{1,0},{2,1},{3,2},{4,7},{5,4},{6,5},{7,6},{8,11},{9,8},{10,9... | collective-permute-start | bytes 1622024 | tf_op jit(solution)/shard_map/ppermute | solution.py:291
  53.7 0.0 copy-done.3
  53.7 0.3 gate_columns.1.columns
  54.1 0.0 copy-start.2
  54.1 1.0 copy-done.2
  55.0 0.6 all-to-all-done.source
  55.7 0.0 copy-start.6
  55.7 1.2 %copy-done.6 = bf16[16,3,128,128]{3,2,1,0:T(8,128)(2,1)} copy-done((bf16[16,3,128,128]{3,2,1,0:T(8,128)(2,1)}, bf16[16,3,128,128]{3,2,1,0:T(8,128)(2,1)S(1)}, u32[]{:S(2)}) %copy-start.6) | copy-done | bytes 1572888
  56.9 14.1 %attend.1.after = bf16[16,64,256]{2,1,0:T(8,128)(2,1)} custom-call(bf16[16,3,128,128]{3,2,1,0:T(8,128)(2,1)} %copy-done.6, bf16[4096,128]{1,0:T(8,128)(2,1)} %copy-done.2), custom_call_target="tpu_custom_call" | custom-call | flops 10000000000 | bytes 4000000 | tf_op jit(solution)/shard_map/attend/pallas_call | solution.py:194
  71.0 0.0 copy-done.4
  71.0 0.0 collective-permute-done.refs_1_
  71.0 0.0 copy-start.7
  71.0 0.0 collective-permute-done.1.refs_2_
  71.0 0.0 copy-start.8
  71.0 3.6 %collective-permute-done.2.refs_3_ = bf16[12,44,512]{2,1,0:T(8,128)(2,1)} collective-permute-done((bf16[12,44,512]{2,1,0:T(8,128)(2,1)S(1)}, bf16[12,44,512]{2,1,0:T(8,128)(2,1)}, u32[]{:S(2)}, u32[]{:S(2)}) %collective-permute-start.2) | collective-permute-done | bytes 540704 | tf_op jit(solution)/shard_map/ppermute | solution.py:291
  74.7 0.0 copy-done.7
  74.7 0.0 copy-done.8
  74.7 0.0 copy-start.5
  74.7 3.6 %assemble.1.mine = bf16[2112,512]{1,0:T(8,128)(2,1)} custom-call(s32[1]{0:T(128)} %bitcast.5.me, bf16[16,64,256]{2,1,0:T(8,128)(2,1)} %attend.1.after, bf16[12,44,512]{2,1,0:T(8,128)(2,1)} %copy-done.4, bf16[12,44,512]{2,1,0:T(8,128)(2,1)} %copy-done.7, bf16[12,44,512]{2,1,0:T(8,128)(2,1)} %copy-done.8, bf16[12,44,512]{2,1,0:T(8,128)(2,1)} %collective-permute-done.2.refs_3_), custom_call_target="tpu_custom_call" | custom-call | flops 1000000 | bytes 4300000 | tf_op jit(solution)/shard_map/assemble/pallas_call | solution.py:236
  78.2 4.5 %collective-permute-start.3 = (bf16[2112,512]{1,0:T(8,128)(2,1)}, bf16[2112,512]{1,0:T(8,128)(2,1)S(1)}, u32[]{:S(2)}, u32[]{:S(2)}) collective-permute-start(bf16[2112,512]{1,0:T(8,128)(2,1)} %assemble.1.mine), channel_id=1, source_target_pairs={{0,48},{48,0},{1,49},{49,1},{2,50},{50,2},{3,51},{51,3},{4,52},{52... | collective-permute-start | bytes 6488072 | tf_op jit(solution)/shard_map/ppermute | solution.py:296
  82.8 0.0 copy-done.5
  82.8 24.2 %all_to_all.10.attended = bf16[16,64,256]{2,1,0:T(8,128)(2,1)S(1)} all-to-all(bf16[16,64,256]{2,1,0:T(8,128)(2,1)S(1)} %copy-done.5), channel_id=1, replica_groups=mesh['sp_0'=8,'sp_1'=2,'z'=12,'x'=4] {'sp_0','sp_1'}, dimensions={0} | all-to-all | bytes 1048576 | tf_op jit(solution)/shard_map/all_to_all | solution.py:297
  107.0 0.0 collective-permute-done.3.other
  107.0 0.0 copy-start.1
  107.0 1.6 %copy-done.1 = bf16[2112,512]{1,0:T(8,128)(2,1)S(1)} copy-done((bf16[2112,512]{1,0:T(8,128)(2,1)S(1)}, bf16[2112,512]{1,0:T(8,128)(2,1)}, u32[]{:S(2)}) %copy-start.1) | copy-done | bytes 2162712
  108.6 3.4 %project.1 = bf16[2112,256]{1,0:T(8,128)(2,1)} custom-call(s32[1]{0:T(128)} %bitcast.core, bf16[16,64,256]{2,1,0:T(8,128)(2,1)S(1)} %all_to_all.10.attended, bf16[2112,512]{1,0:T(8,128)(2,1)S(1)} %copy-done.1, bf16[2112,512]{1,0:T(8,128)(2,1)S(1)} %collective-permute-done.3.other), custom_call_target="tpu_custom_call" | custom-call | flops 1100000000 | bytes 6000000 | tf_op jit(solution)/shard_map/project/pallas_call | solution.py:261
  (1 shorter events, 0.0 us)
Async XLA Ops:
  0.0 17.1 %copy-start = (bf16[1024,44]{0,1:T(8,128)(2,1)S(1)}, bf16[1024,44]{0,1:T(8,128)(2,1)}, u32[]{:S(2)}) copy-start(bf16[1024,44]{0,1:T(8,128)(2,1)} %param.9) | copy-start | bytes 270340
  3.1 50.6 %copy-start.3 = (f32[1,1,4096]{2,1,0:T(1,128)S(1)}, f32[1,1,4096]{2,1,0:T(1,128)}, u32[]{:S(2)}) copy-start(f32[1,1,4096]{2,1,0:T(1,128)} %param.8) | copy-start | bytes 49156
  3.1 52.6 %all-to-all-start = ((bf16[16,3,128,128]{3,2,1,0:T(8,128)(2,1)}), bf16[16,3,128,128]{3,2,1,0:T(8,128)(2,1)S(1)}, u32[]{:S(2)}, u32[]{:S(2)}) async-start(bf16[16,3,128,128]{3,2,1,0:T(8,128)(2,1)} %pack.1), calls=%async_computation | async-start | bytes 3145728 | tf_op jit(solution)/shard_map/all_to_all | solution.py:283
  43.2 27.8 %copy-start.4 = (bf16[12,44,512]{2,1,0:T(8,128)(2,1)}, bf16[12,44,512]{2,1,0:T(8,128)(2,1)S(1)}, u32[]{:S(2)}) copy-start(bf16[12,44,512]{2,1,0:T(8,128)(2,1)S(1)} %all-gather.1.refs_0_) | copy-start | bytes 1622020
  43.2 27.8 %collective-permute-start = (bf16[12,44,512]{2,1,0:T(8,128)(2,1)S(1)}, bf16[12,44,512]{2,1,0:T(8,128)(2,1)S(1)}, u32[]{:S(2)}, u32[]{:S(2)}) collective-permute-start(bf16[12,44,512]{2,1,0:T(8,128)(2,1)S(1)} %all-gather.1.refs_0_), channel_id=1, source_target_pairs={{0,1},{1,2},{2,3},{3,0},{4,5},{5,6},{6,7},{7,4},{8,9},{9,10},{10,1... | collective-permute-start | bytes 1622024 | tf_op jit(solution)/shard_map/ppermute | solution.py:291
  46.3 24.7 %collective-permute-start.1 = (bf16[12,44,512]{2,1,0:T(8,128)(2,1)S(1)}, bf16[12,44,512]{2,1,0:T(8,128)(2,1)S(1)}, u32[]{:S(2)}, u32[]{:S(2)}) collective-permute-start(bf16[12,44,512]{2,1,0:T(8,128)(2,1)S(1)} %all-gather.1.refs_0_), channel_id=1, source_target_pairs={{0,2},{1,3},{2,0},{3,1},{4,6},{5,7},{6,4},{7,5},{8,10},{9,11},{10,... | collective-permute-start | bytes 1622024 | tf_op jit(solution)/shard_map/ppermute | solution.py:291
  50.7 24.0 %collective-permute-start.2 = (bf16[12,44,512]{2,1,0:T(8,128)(2,1)S(1)}, bf16[12,44,512]{2,1,0:T(8,128)(2,1)}, u32[]{:S(2)}, u32[]{:S(2)}) collective-permute-start(bf16[12,44,512]{2,1,0:T(8,128)(2,1)S(1)} %all-gather.1.refs_0_), channel_id=1, source_target_pairs={{0,3},{1,0},{2,1},{3,2},{4,7},{5,4},{6,5},{7,6},{8,11},{9,8},{10,9... | collective-permute-start | bytes 1622024 | tf_op jit(solution)/shard_map/ppermute | solution.py:291
  54.1 1.0 copy-start.2
  55.7 1.2 %copy-start.6 = (bf16[16,3,128,128]{3,2,1,0:T(8,128)(2,1)}, bf16[16,3,128,128]{3,2,1,0:T(8,128)(2,1)S(1)}, u32[]{:S(2)}) copy-start(bf16[16,3,128,128]{3,2,1,0:T(8,128)(2,1)S(1)} %all-to-all-done.source) | copy-start | bytes 4718596
  71.0 3.6 %copy-start.7 = (bf16[12,44,512]{2,1,0:T(8,128)(2,1)}, bf16[12,44,512]{2,1,0:T(8,128)(2,1)S(1)}, u32[]{:S(2)}) copy-start(bf16[12,44,512]{2,1,0:T(8,128)(2,1)S(1)} %collective-permute-done.refs_1_) | copy-start | bytes 1622020
  71.0 3.6 %copy-start.8 = (bf16[12,44,512]{2,1,0:T(8,128)(2,1)}, bf16[12,44,512]{2,1,0:T(8,128)(2,1)S(1)}, u32[]{:S(2)}) copy-start(bf16[12,44,512]{2,1,0:T(8,128)(2,1)S(1)} %collective-permute-done.1.refs_2_) | copy-start | bytes 1622020
  74.7 8.1 %copy-start.5 = (bf16[16,64,256]{2,1,0:T(8,128)(2,1)S(1)}, bf16[16,64,256]{2,1,0:T(8,128)(2,1)}, u32[]{:S(2)}) copy-start(bf16[16,64,256]{2,1,0:T(8,128)(2,1)} %attend.1.after) | copy-start | bytes 1572868
  78.2 28.8 %collective-permute-start.3 = (bf16[2112,512]{1,0:T(8,128)(2,1)}, bf16[2112,512]{1,0:T(8,128)(2,1)S(1)}, u32[]{:S(2)}, u32[]{:S(2)}) collective-permute-start(bf16[2112,512]{1,0:T(8,128)(2,1)} %assemble.1.mine), channel_id=1, source_target_pairs={{0,48},{48,0},{1,49},{49,1},{2,50},{50,2},{3,51},{51,3},{4,52},{52... | collective-permute-start | bytes 6488072 | tf_op jit(solution)/shard_map/ppermute | solution.py:296
  107.0 1.6 %copy-start.1 = (bf16[2112,512]{1,0:T(8,128)(2,1)S(1)}, bf16[2112,512]{1,0:T(8,128)(2,1)}, u32[]{:S(2)}) copy-start(bf16[2112,512]{1,0:T(8,128)(2,1)} %assemble.1.mine) | copy-start | bytes 6488068

commit v3 on v2

--- a/solution.py
+++ b/solution.py
@@ -111,28 +111,12 @@
     )(gate)
 
 
-def attend_kernel(source, columns, out, parts, gate, keys, values, logits, finished, arrived, left):
+def attend_kernel(parts, gate, out, keys, values, logits):
     count = parts.shape[0]
-
-    def arrival(b):
-        rows = slice(256 * b, 256 * b + 256)
-        return (
-            pltpu.make_async_copy(source.at[b], parts.at[b], arrived.at[b, 0]),
-            pltpu.make_async_copy(columns.at[rows], gate.at[rows], arrived.at[b, 1]),
-        )
-
-    def departure(b):
-        return pltpu.make_async_copy(finished.at[b], out.at[b], left.at[b])
-
-    for b in range(count):
-        for copy in arrival(b):
-            copy.start()
     lanes = low_lanes((128, 128))
     values[64:80, :] = jnp.ones((16, values.shape[1]), jnp.bfloat16)
     for b in range(count):
         base = 256 * b
-        for copy in arrival(b):
-            copy.wait()
         k = parts[b, 1]
         swapped = swap_halves(k)
         keys[base : base + 128, 0:128] = jnp.where(lanes, k, swapped)
@@ -176,16 +160,13 @@
                 values[:, 256 * j : 256 * j + 256], p, preferred_element_type=jnp.float32
             )
             total = o if total is None else total + o
-        finished[i] = (total[:64] / total[64:65]).astype(jnp.bfloat16)
-        departure(i).start()
+        out[i] = (total[:64] / total[64:65]).astype(jnp.bfloat16)
 
     peak = first(0)
     for i in range(count):
         following = first(i + 1) if i + 1 < count else None
         second(i, peak)
         peak = following
-    for i in range(count):
-        departure(i).wait()
 
 
 def attend(parts, gate):
@@ -194,19 +175,14 @@
     return pl.pallas_call(
         attend_kernel,
         out_shape=jax.ShapeDtypeStruct((count, 64, 256), jnp.bfloat16),
-        in_specs=[HBM, HBM],
-        out_specs=HBM,
+        in_specs=[VMEM] * 2,
+        out_specs=VMEM,
         scratch_shapes=[
-            pltpu.VMEM(parts.shape, jnp.bfloat16),
-            pltpu.VMEM(gate.shape, jnp.bfloat16),
             pltpu.VMEM((length, 256), jnp.bfloat16),
             pltpu.VMEM((80, length), jnp.bfloat16),
             pltpu.VMEM((2, length, 256), jnp.float32),
-            pltpu.VMEM((count, 64, 256), jnp.bfloat16),
-            pltpu.SemaphoreType.DMA((count, 2)),
-            pltpu.SemaphoreType.DMA((count,)),
         ],
-        compiler_params=pltpu.CompilerParams(vmem_limit_bytes=60 * 2**20),
+        compiler_params=pltpu.CompilerParams(vmem_limit_bytes=32 * 2**20),
         cost_estimate=pl.CostEstimate(
             flops=10_000_000_000, bytes_accessed=4_000_000, transcendentals=9_000_000
         ),
@@ -238,7 +214,7 @@
         out_shape=jax.ShapeDtypeStruct((len(blocks) * groups * columns, depth), jnp.bfloat16),
         in_specs=[SMEM, pl.BlockSpec(memory_space=pl.ANY)] + [VMEM] * len(blocks),
         out_specs=VMEM,
-        compiler_params=pltpu.CompilerParams(vmem_limit_bytes=60 * 2**20),
+        compiler_params=pltpu.CompilerParams(vmem_limit_bytes=16 * 2**20),
         cost_estimate=pl.CostEstimate(flops=1_000_000, bytes_accessed=4_300_000, transcendentals=0),
         name="assemble",
     )(me, after, *blocks)

time: 113 us -> 109 us (0.965)
  waiting for transfers between devices: 4.26 us -> 9.34 us
  Pallas kernels: 24.6 us -> 20.1 us
  local copies, waits for them, and re-layouts: 3.78 us -> 0.02 us
    ppermute x3, waiting for transfers between devices: 3.62 us -> 7.72 us  [body(): lax.ppermute(along_z, 'x', [(i, (i + hop) % n) for i in range(n)])]
    unnamed x19 -> x5, local copies, waits for them, and re-layouts: 3.78 us -> 0.02 us
    pallas_call x1, Pallas kernels: 14.1 us -> 11.2 us  [attend(): pl.pallas_call(attend_kernel, out_shape=jax.ShapeDtypeStruct((count, 64,...]
    pallas_call x1, Pallas kernels: 3.56 us -> 1.97 us  [assemble(): pl.pallas_call(assemble_kernel, out_shape=jax.ShapeDtypeStruct((len(block...]
  transfers between devices with their start and end apart: 5 -> 5, of which waited for: 2 -> 3; matrix products, arithmetic and copies ran while one was open for 0% -> 0% of each run, Pallas kernels for 13% -> 11%
where the time goes in v3:
time: 109 us
  blocking collectives  50.3 us (46%)
  starting transfers between devices  29.1 us (27%)
  Pallas kernels  20.1 us (18%)
  waiting for transfers between devices  9.34 us (9%)
    all_gather x1, blocking collectives, body(): along_z = lax.all_gather(own[None], 'z', axis=0, tiled=True)  26 us
    all_to_all x1, blocking collectives, body(): back = lax.all_to_all(local, SP, 0, 0, tiled=True)  24.2 us
    all_to_all x1, starting transfers between devices, body(): parts = lax.all_to_all(packed, SP, 0, 0, tiled=True)  14 us
    pallas_call x1, Pallas kernels, attend(): pl.pallas_call(attend_kernel, out_shape=jax.ShapeDtypeStruct((count, 64,...  11.2 us
    ppermute x3, starting transfers between devices, body(): lax.ppermute(along_z, 'x', [(i, (i + hop) % n) for i in range(n)])  10.5 us
    ppermute x3, waiting for transfers between devices, body(): lax.ppermute(along_z, 'x', [(i, (i + hop) % n) for i in range(n)])  7.72 us
    ppermute x1, starting transfers between devices, body(): other = lax.ppermute(mine, 'sp_1', [(0, 1), (1, 0)])  4.55 us
    pallas_call x1, Pallas kernels, project(): pl.pallas_call(project_kernel, out_shape=jax.ShapeDtypeStruct((columns, a...  3.45 us
  transfers between devices with their start and end apart: 5, of which 3 were waited for; matrix products, arithmetic and copies ran while one was open for 0% of the time, Pallas kernels for 11%

profile of v3, /device:TPU:1, one launch (start us, length us, event | category | flops | bytes accessed | tf_op | source)
XLA Modules:
  0.0 108.9 jit_solution(13374729403517710169)
XLA Ops:
  0.0 0.0 copy-start
  0.0 3.1 %pack.1 = bf16[16,3,128,128]{3,2,1,0:T(8,128)(2,1)} custom-call(bf16[256,1024]{1,0:T(8,128)(2,1)} %bitcast.14, bf16[256,1024]{1,0:T(8,128)(2,1)} %bitcast.15, bf16[256,1024]{1,0:T(8,128)(2,1)} %bitcast.16), custom_call_target="tpu_custom_call" | custom-call | flops 1000000 | bytes 3000000 | tf_op jit(solution)/shard_map/pack/pallas_call | solution.py:70
  3.1 0.0 copy-start.1
  3.1 14.0 %all-to-all-start = ((bf16[16,3,128,128]{3,2,1,0:T(8,128)(2,1)}), bf16[16,3,128,128]{3,2,1,0:T(8,128)(2,1)S(1)}, u32[]{:S(2)}, u32[]{:S(2)}) async-start(bf16[16,3,128,128]{3,2,1,0:T(8,128)(2,1)} %pack.1), calls=%async_computation | async-start | bytes 3145728 | tf_op jit(solution)/shard_map/all_to_all | solution.py:259
  17.1 0.0 copy-done
  17.1 26.0 %all-gather.1.refs_0_ = bf16[12,44,512]{2,1,0:T(8,128)(2,1)S(1)} all-gather(bf16[1,44,512]{2,1,0:T(8,128)(2,1)S(1)} %dynamic-slice_bitcast_fusion), channel_id=2, replica_groups=mesh['sp_0'=8,'sp_1'=2,'z'=12,'x'=4] {'z'}, dimensions={0}, use_global_device_ids=true | all-gather | bytes 585728 | tf_op jit(solution)/shard_map/all_gather | solution.py:264
  43.2 3.1 %collective-permute-start = (bf16[12,44,512]{2,1,0:T(8,128)(2,1)S(1)}, bf16[12,44,512]{2,1,0:T(8,128)(2,1)}, u32[]{:S(2)}, u32[]{:S(2)}) collective-permute-start(bf16[12,44,512]{2,1,0:T(8,128)(2,1)S(1)} %all-gather.1.refs_0_), channel_id=1, source_target_pairs={{0,1},{1,2},{2,3},{3,0},{4,5},{5,6},{6,7},{7,4},{8,9},{9,10},{10,1... | collective-permute-start | bytes 1622024 | tf_op jit(solution)/shard_map/ppermute | solution.py:267
  46.3 4.4 %collective-permute-start.1 = (bf16[12,44,512]{2,1,0:T(8,128)(2,1)S(1)}, bf16[12,44,512]{2,1,0:T(8,128)(2,1)}, u32[]{:S(2)}, u32[]{:S(2)}) collective-permute-start(bf16[12,44,512]{2,1,0:T(8,128)(2,1)S(1)} %all-gather.1.refs_0_), channel_id=1, source_target_pairs={{0,2},{1,3},{2,0},{3,1},{4,6},{5,7},{6,4},{7,5},{8,10},{9,11},{10,... | collective-permute-start | bytes 1622024 | tf_op jit(solution)/shard_map/ppermute | solution.py:267
  50.6 3.1 %collective-permute-start.2 = (bf16[12,44,512]{2,1,0:T(8,128)(2,1)S(1)}, bf16[12,44,512]{2,1,0:T(8,128)(2,1)}, u32[]{:S(2)}, u32[]{:S(2)}) collective-permute-start(bf16[12,44,512]{2,1,0:T(8,128)(2,1)S(1)} %all-gather.1.refs_0_), channel_id=1, source_target_pairs={{0,3},{1,0},{2,1},{3,2},{4,7},{5,4},{6,5},{7,6},{8,11},{9,8},{10,9... | collective-permute-start | bytes 1622024 | tf_op jit(solution)/shard_map/ppermute | solution.py:267
  53.7 0.0 copy-done.1
  53.7 0.3 gate_columns.1.gate
  54.1 1.6 %all-to-all-done.parts = bf16[16,3,128,128]{3,2,1,0:T(8,128)(2,1)S(1)} async-done(((bf16[16,3,128,128]{3,2,1,0:T(8,128)(2,1)}), bf16[16,3,128,128]{3,2,1,0:T(8,128)(2,1)S(1)}, u32[]{:S(2)}, u32[]{:S(2)}) %all-to-all-start) | async-done | bytes 1572896 | tf_op jit(solution)/shard_map/all_to_all | solution.py:259
  55.7 11.2 %attend.1.after = bf16[16,64,256]{2,1,0:T(8,128)(2,1)S(1)} custom-call(bf16[16,3,128,128]{3,2,1,0:T(8,128)(2,1)S(1)} %all-to-all-done.parts, bf16[4096,128]{1,0:T(8,128)(2,1)S(1)} %gate_columns.1.gate), custom_call_target="tpu_custom_call" | custom-call | flops 10000000000 | bytes 4000000 | tf_op jit(solution)/shard_map/attend/pallas_call | solution.py:175
  66.9 0.0 collective-permute-done.refs_1_
  66.9 3.3 %collective-permute-done.1.refs_2_ = bf16[12,44,512]{2,1,0:T(8,128)(2,1)} collective-permute-done((bf16[12,44,512]{2,1,0:T(8,128)(2,1)S(1)}, bf16[12,44,512]{2,1,0:T(8,128)(2,1)}, u32[]{:S(2)}, u32[]{:S(2)}) %collective-permute-start.1) | collective-permute-done | bytes 540704 | tf_op jit(solution)/shard_map/ppermute | solution.py:267
  70.2 4.4 %collective-permute-done.2.refs_3_ = bf16[12,44,512]{2,1,0:T(8,128)(2,1)} collective-permute-done((bf16[12,44,512]{2,1,0:T(8,128)(2,1)S(1)}, bf16[12,44,512]{2,1,0:T(8,128)(2,1)}, u32[]{:S(2)}, u32[]{:S(2)}) %collective-permute-start.2) | collective-permute-done | bytes 540704 | tf_op jit(solution)/shard_map/ppermute | solution.py:267
  74.6 2.0 %assemble.1.mine = bf16[2112,512]{1,0:T(8,128)(2,1)S(1)} custom-call(s32[1]{0:T(128)} %bitcast.5.me, bf16[16,64,256]{2,1,0:T(8,128)(2,1)S(1)} %attend.1.after, bf16[12,44,512]{2,1,0:T(8,128)(2,1)S(1)} %all-gather.1.refs_0_, bf16[12,44,512]{2,1,0:T(8,128)(2,1)} %collective-permute-done.refs_1_, bf16[12,44,512]{2,1,0:T(8,128)(2,1)} %collective-permute-done.1.refs_2_, ...), custom_call_target="tpu_custom_call" | custom-call | flops 1000000 | bytes 4300000 | tf_op jit(solution)/shard_map/assemble/pallas_call | solution.py:212
  76.6 4.5 %collective-permute-start.3 = (bf16[2112,512]{1,0:T(8,128)(2,1)S(1)}, bf16[2112,512]{1,0:T(8,128)(2,1)S(1)}, u32[]{:S(2)}, u32[]{:S(2)}) collective-permute-start(bf16[2112,512]{1,0:T(8,128)(2,1)S(1)} %assemble.1.mine), channel_id=1, source_target_pairs={{0,48},{48,0},{1,49},{49,1},{2,50},{50,2},{3,51},{51,3},{4,52},{52... | collective-permute-start | bytes 6488072 | tf_op jit(solution)/shard_map/ppermute | solution.py:272
  81.2 24.2 %all_to_all.10.attended = bf16[16,64,256]{2,1,0:T(8,128)(2,1)S(1)} all-to-all(bf16[16,64,256]{2,1,0:T(8,128)(2,1)S(1)} %attend.1.after), channel_id=1, replica_groups=mesh['sp_0'=8,'sp_1'=2,'z'=12,'x'=4] {'sp_0','sp_1'}, dimensions={0} | all-to-all | bytes 1048576 | tf_op jit(solution)/shard_map/all_to_all | solution.py:273
  105.4 0.0 collective-permute-done.3.other
  105.4 3.4 %project.1 = bf16[2112,256]{1,0:T(8,128)(2,1)} custom-call(s32[1]{0:T(128)} %bitcast.core, bf16[16,64,256]{2,1,0:T(8,128)(2,1)S(1)} %all_to_all.10.attended, bf16[2112,512]{1,0:T(8,128)(2,1)S(1)} %assemble.1.mine, bf16[2112,512]{1,0:T(8,128)(2,1)S(1)} %collective-permute-done.3.other), custom_call_target="tpu_custom_call" | custom-call | flops 1100000000 | bytes 6000000 | tf_op jit(solution)/shard_map/project/pallas_call | solution.py:237
  (1 shorter events, 0.0 us)
Async XLA Ops:
  0.0 17.1 %copy-start = (bf16[1024,44]{0,1:T(8,128)(2,1)S(1)}, bf16[1024,44]{0,1:T(8,128)(2,1)}, u32[]{:S(2)}) copy-start(bf16[1024,44]{0,1:T(8,128)(2,1)} %param.9) | copy-start | bytes 270340
  3.1 50.6 %copy-start.1 = (f32[1,1,4096]{2,1,0:T(1,128)S(1)}, f32[1,1,4096]{2,1,0:T(1,128)}, u32[]{:S(2)}) copy-start(f32[1,1,4096]{2,1,0:T(1,128)} %param.8) | copy-start | bytes 49156
  3.1 52.6 %all-to-all-start = ((bf16[16,3,128,128]{3,2,1,0:T(8,128)(2,1)}), bf16[16,3,128,128]{3,2,1,0:T(8,128)(2,1)S(1)}, u32[]{:S(2)}, u32[]{:S(2)}) async-start(bf16[16,3,128,128]{3,2,1,0:T(8,128)(2,1)} %pack.1), calls=%async_computation | async-start | bytes 3145728 | tf_op jit(solution)/shard_map/all_to_all | solution.py:259
  43.2 23.8 %collective-permute-start = (bf16[12,44,512]{2,1,0:T(8,128)(2,1)S(1)}, bf16[12,44,512]{2,1,0:T(8,128)(2,1)}, u32[]{:S(2)}, u32[]{:S(2)}) collective-permute-start(bf16[12,44,512]{2,1,0:T(8,128)(2,1)S(1)} %all-gather.1.refs_0_), channel_id=1, source_target_pairs={{0,1},{1,2},{2,3},{3,0},{4,5},{5,6},{6,7},{7,4},{8,9},{9,10},{10,1... | collective-permute-start | bytes 1622024 | tf_op jit(solution)/shard_map/ppermute | solution.py:267
  46.3 24.0 %collective-permute-start.1 = (bf16[12,44,512]{2,1,0:T(8,128)(2,1)S(1)}, bf16[12,44,512]{2,1,0:T(8,128)(2,1)}, u32[]{:S(2)}, u32[]{:S(2)}) collective-permute-start(bf16[12,44,512]{2,1,0:T(8,128)(2,1)S(1)} %all-gather.1.refs_0_), channel_id=1, source_target_pairs={{0,2},{1,3},{2,0},{3,1},{4,6},{5,7},{6,4},{7,5},{8,10},{9,11},{10,... | collective-permute-start | bytes 1622024 | tf_op jit(solution)/shard_map/ppermute | solution.py:267
  50.6 24.0 %collective-permute-start.2 = (bf16[12,44,512]{2,1,0:T(8,128)(2,1)S(1)}, bf16[12,44,512]{2,1,0:T(8,128)(2,1)}, u32[]{:S(2)}, u32[]{:S(2)}) collective-permute-start(bf16[12,44,512]{2,1,0:T(8,128)(2,1)S(1)} %all-gather.1.refs_0_), channel_id=1, source_target_pairs={{0,3},{1,0},{2,1},{3,2},{4,7},{5,4},{6,5},{7,6},{8,11},{9,8},{10,9... | collective-permute-start | bytes 1622024 | tf_op jit(solution)/shard_map/ppermute | solution.py:267
  76.6 28.8 %collective-permute-start.3 = (bf16[2112,512]{1,0:T(8,128)(2,1)S(1)}, bf16[2112,512]{1,0:T(8,128)(2,1)S(1)}, u32[]{:S(2)}, u32[]{:S(2)}) collective-permute-start(bf16[2112,512]{1,0:T(8,128)(2,1)S(1)} %assemble.1.mine), channel_id=1, source_target_pairs={{0,48},{48,0},{1,49},{49,1},{2,50},{50,2},{3,51},{51,3},{4,52},{52... | collective-permute-start | bytes 6488072 | tf_op jit(solution)/shard_map/ppermute | solution.py:272

commit v4 on v3

--- a/solution.py
+++ b/solution.py
@@ -214,43 +214,90 @@
         out_shape=jax.ShapeDtypeStruct((len(blocks) * groups * columns, depth), jnp.bfloat16),
         in_specs=[SMEM, pl.BlockSpec(memory_space=pl.ANY)] + [VMEM] * len(blocks),
         out_specs=VMEM,
-        compiler_params=pltpu.CompilerParams(vmem_limit_bytes=16 * 2**20),
+        compiler_params=pltpu.CompilerParams(vmem_limit_bytes=60 * 2**20),
         cost_estimate=pl.CostEstimate(flops=1_000_000, bytes_accessed=4_300_000, transcendentals=0),
         name="assemble",
     )(me, after, *blocks)
 
 
-def project_kernel(core, attended, mine, other, out):
+def settle_kernel(source, out):
+    del source, out
+
+
+def settle(a):
+    return pl.pallas_call(
+        settle_kernel,
+        out_shape=jax.ShapeDtypeStruct(a.shape, a.dtype),
+        in_specs=[HBM],
+        out_specs=HBM,
+        input_output_aliases={0: 0},
+        compiler_params=pltpu.CompilerParams(vmem_limit_bytes=60 * 2**20),
+        cost_estimate=pl.CostEstimate(flops=1_000_000, bytes_accessed=8_600_000, transcendentals=0),
+        name="settle",
+    )(a)
+
+
+def project_kernel(core, back, mine, other, out, attended, weight, finished, arrived, left):
     heads, depth, rows = attended.shape
     c, half = core[0], heads // 2
-
-    def columns(first):
-        return attended[pl.ds(first, half)].reshape(half * depth, rows)
-
-    total = jnp.dot(mine[...], columns(c * half), preferred_element_type=jnp.float32)
-    total += jnp.dot(other[...], columns((1 - c) * half), preferred_element_type=jnp.float32)
-    out[...] = total.astype(jnp.bfloat16)
-
-
-def project(core, attended, mine, other):
-    columns, step = mine.shape[0], 352
+    steps = left.shape[0]
+    step = out.shape[0] // steps
+
+    def block(n):
+        return slice(step * n, step * n + step)
+
+    def arrival(n):
+        return [
+            pltpu.make_async_copy(source.at[block(n)], weight.at[k, block(n)], arrived.at[n, k])
+            for k, source in enumerate((mine, other))
+        ]
+
+    def departure(n):
+        return pltpu.make_async_copy(finished.at[block(n)], out.at[block(n)], left.at[n])
+
+    whole = pltpu.make_async_copy(back, attended, arrived.at[steps, 0])
+    whole.start()
+    for n in range(steps):
+        for copy in arrival(n):
+            copy.start()
+    whole.wait()
+    halves = [
+        attended[pl.ds(first, half)].reshape(half * depth, rows)
+        for first in (c * half, (1 - c) * half)
+    ]
+    for n in range(steps):
+        total = None
+        for k, copy in enumerate(arrival(n)):
+            copy.wait()
+            part = jnp.dot(weight[k, block(n), :], halves[k], preferred_element_type=jnp.float32)
+            total = part if total is None else total + part
+        finished[block(n), :] = total.astype(jnp.bfloat16)
+        departure(n).start()
+    for n in range(steps):
+        departure(n).wait()
+
+
+def project(core, back, mine, other):
+    columns, depth = mine.shape
+    rows, steps = back.shape[2], 6
     return pl.pallas_call(
         project_kernel,
-        out_shape=jax.ShapeDtypeStruct((columns, attended.shape[2]), jnp.bfloat16),
-        grid=(columns // step,),
-        in_specs=[
-            SMEM,
-            pl.BlockSpec(attended.shape, lambda i: (0, 0, 0)),
-            pl.BlockSpec((step, mine.shape[1]), lambda i: (i, 0)),
-            pl.BlockSpec((step, other.shape[1]), lambda i: (i, 0)),
+        out_shape=jax.ShapeDtypeStruct((columns, rows), jnp.bfloat16),
+        in_specs=[SMEM] + [HBM] * 3,
+        out_specs=HBM,
+        scratch_shapes=[
+            pltpu.VMEM(back.shape, jnp.bfloat16),
+            pltpu.VMEM((2, columns, depth), jnp.bfloat16),
+            pltpu.VMEM((columns, rows), jnp.bfloat16),
+            pltpu.SemaphoreType.DMA((steps + 1, 2)),
+            pltpu.SemaphoreType.DMA((steps,)),
         ],
-        out_specs=pl.BlockSpec((step, attended.shape[2]), lambda i: (i, 0)),
-        compiler_params=pltpu.CompilerParams(vmem_limit_bytes=16 * 2**20),
+        compiler_params=pltpu.CompilerParams(vmem_limit_bytes=60 * 2**20),
         cost_estimate=pl.CostEstimate(
             flops=1_100_000_000, bytes_accessed=6_000_000, transcendentals=0
         ),
         name="project",
-    )(core, attended, mine, other)
+    )(core, back, mine, other)
 
 
 def body(queries, keys, values, cum_gate, out_weight):
@@ -270,6 +317,7 @@
     local = attend(parts, gate)
     mine = assemble(x.reshape(1), local, blocks)
     other = lax.ppermute(mine, "sp_1", [(0, 1), (1, 0)])
+    other = settle(other)
     back = lax.all_to_all(local, SP, 0, 0, tiled=True)
     return project(core.reshape(1), back, mine, other).T[None]
 

time: 109 us -> 116 us (1.064)
  blocking collectives: 50.3 us -> 26 us
  waiting for transfers between devices: 9.34 us -> 29.8 us
  Pallas kernels: 20.1 us -> 24.3 us
  starting transfers between devices: 29.1 us -> 32.9 us
  local copies, waits for them, and re-layouts: 0.02 us -> 2.15 us
    all_to_all x1 -> x0, blocking collectives: 24.2 us -> none  [body(): back = lax.all_to_all(local, SP, 0, 0, tiled=True)]
    all_to_all x0 -> x1, waiting for transfers between devices: none -> 15.9 us  [body(): back = lax.all_to_all(local, SP, 0, 0, tiled=True)]
    all_to_all x0 -> x1, starting transfers between devices: none -> 7.1 us  [body(): back = lax.all_to_all(local, SP, 0, 0, tiled=True)]
    ppermute x3, waiting for transfers between devices: 7.72 us -> 11.1 us  [body(): lax.ppermute(along_z, 'x', [(i, (i + hop) % n) for i in range(n)])]
    unnamed x5 -> x11, local copies, waits for them, and re-layouts: 0.02 us -> 2.15 us
    ppermute x1, starting transfers between devices: 4.55 us -> 2.54 us  [body(): other = lax.ppermute(mine, 'sp_1', [(0, 1), (1, 0)])]
    pallas_call x1 -> x2, Pallas kernels: 3.45 us -> 5.34 us  [the longest x1 5.34 us: project(): pl.pallas_call(project_kernel, out_shape=jax.ShapeDtypeStruct((columns, r...]
    pallas_call x1, Pallas kernels: 1.97 us -> 3.5 us  [assemble(): pl.pallas_call(assemble_kernel, out_shape=jax.ShapeDtypeStruct((len(block...]
  transfers between devices with their start and end apart: 5 -> 6, of which waited for: 3 -> 3; matrix products, arithmetic and copies ran while one was open for 0% -> 0% of each run, Pallas kernels for 11% -> 11%
where the time goes in v4:
time: 116 us; the launch traced here: 115 us
  starting transfers between devices  32.9 us (28%)
  waiting for transfers between devices  29.8 us (26%)
  blocking collectives  26 us (22%)
  Pallas kernels  24.3 us (21%)
  local copies, waits for them, and re-layouts  2.15 us (2%)
    all_gather x1, blocking collectives, body(): along_z = lax.all_gather(own[None], 'z', axis=0, tiled=True)  26 us
    all_to_all x1, waiting for transfers between devices, body(): back = lax.all_to_all(local, SP, 0, 0, tiled=True)  15.9 us
    all_to_all x1, starting transfers between devices, body(): parts = lax.all_to_all(packed, SP, 0, 0, tiled=True)  14 us
    pallas_call x1, Pallas kernels, attend(): pl.pallas_call(attend_kernel, out_shape=jax.ShapeDtypeStruct((count, 64,...  12 us
    ppermute x3, waiting for transfers between devices, body(): lax.ppermute(along_z, 'x', [(i, (i + hop) % n) for i in range(n)])  11.1 us
    ppermute x3, starting transfers between devices, body(): lax.ppermute(along_z, 'x', [(i, (i + hop) % n) for i in range(n)])  9.32 us
    all_to_all x1, starting transfers between devices, body(): back = lax.all_to_all(local, SP, 0, 0, tiled=True)  7.1 us
    pallas_call x1, Pallas kernels, project(): pl.pallas_call(project_kernel, out_shape=jax.ShapeDtypeStruct((columns, r...  5.34 us
  transfers between devices with their start and end apart: 6, of which 3 were waited for; matrix products, arithmetic and copies ran while one was open for 0% of the time, Pallas kernels for 11%

profile of v4, /device:TPU:1, one launch (start us, length us, event | category | flops | bytes accessed | tf_op | source)
XLA Modules:
  0.0 115.3 jit_solution(16390375972752103835)
XLA Ops:
  0.0 0.0 copy-start
  0.0 3.1 %pack.1 = bf16[16,3,128,128]{3,2,1,0:T(8,128)(2,1)} custom-call(bf16[256,1024]{1,0:T(8,128)(2,1)} %bitcast.14, bf16[256,1024]{1,0:T(8,128)(2,1)} %bitcast.15, bf16[256,1024]{1,0:T(8,128)(2,1)} %bitcast.16), custom_call_target="tpu_custom_call" | custom-call | flops 1000000 | bytes 3000000 | tf_op jit(solution)/shard_map/pack/pallas_call | solution.py:70
  3.1 0.0 copy-start.1
  3.1 14.0 %all-to-all-start = ((bf16[16,3,128,128]{3,2,1,0:T(8,128)(2,1)}), bf16[16,3,128,128]{3,2,1,0:T(8,128)(2,1)S(1)}, u32[]{:S(2)}, u32[]{:S(2)}) async-start(bf16[16,3,128,128]{3,2,1,0:T(8,128)(2,1)} %pack.1), calls=%async_computation | async-start | bytes 3145728 | tf_op jit(solution)/shard_map/all_to_all | solution.py:306
  17.1 0.0 copy-done
  17.1 26.0 %all-gather.1.refs_0_ = bf16[12,44,512]{2,1,0:T(8,128)(2,1)S(1)} all-gather(bf16[1,44,512]{2,1,0:T(8,128)(2,1)S(1)} %dynamic-slice_bitcast_fusion), channel_id=2, replica_groups=mesh['sp_0'=8,'sp_1'=2,'z'=12,'x'=4] {'z'}, dimensions={0}, use_global_device_ids=true | all-gather | bytes 585728 | tf_op jit(solution)/shard_map/all_gather | solution.py:311
  43.2 0.0 copy-start.3
  43.2 4.4 %collective-permute-start.2 = (bf16[12,44,512]{2,1,0:T(8,128)(2,1)S(1)}, bf16[12,44,512]{2,1,0:T(8,128)(2,1)}, u32[]{:S(2)}, u32[]{:S(2)}) collective-permute-start(bf16[12,44,512]{2,1,0:T(8,128)(2,1)S(1)} %all-gather.1.refs_0_), channel_id=1, source_target_pairs={{0,3},{1,0},{2,1},{3,2},{4,7},{5,4},{6,5},{7,6},{8,11},{9,8},{10,9... | collective-permute-start | bytes 1622024 | tf_op jit(solution)/shard_map/ppermute | solution.py:314
  47.6 2.4 %collective-permute-start.1 = (bf16[12,44,512]{2,1,0:T(8,128)(2,1)S(1)}, bf16[12,44,512]{2,1,0:T(8,128)(2,1)}, u32[]{:S(2)}, u32[]{:S(2)}) collective-permute-start(bf16[12,44,512]{2,1,0:T(8,128)(2,1)S(1)} %all-gather.1.refs_0_), channel_id=1, source_target_pairs={{0,2},{1,3},{2,0},{3,1},{4,6},{5,7},{6,4},{7,5},{8,10},{9,11},{10,... | collective-permute-start | bytes 1622024 | tf_op jit(solution)/shard_map/ppermute | solution.py:314
  50.0 2.5 %collective-permute-start = (bf16[12,44,512]{2,1,0:T(8,128)(2,1)S(1)}, bf16[12,44,512]{2,1,0:T(8,128)(2,1)}, u32[]{:S(2)}, u32[]{:S(2)}) collective-permute-start(bf16[12,44,512]{2,1,0:T(8,128)(2,1)S(1)} %all-gather.1.refs_0_), channel_id=1, source_target_pairs={{0,1},{1,2},{2,3},{3,0},{4,5},{5,6},{6,7},{7,4},{8,9},{9,10},{10,1... | collective-permute-start | bytes 1622024 | tf_op jit(solution)/shard_map/ppermute | solution.py:314
  52.5 0.0 copy-done.1
  52.5 0.3 gate_columns.1.gate
  52.9 2.8 %all-to-all-done.parts = bf16[16,3,128,128]{3,2,1,0:T(8,128)(2,1)S(1)} async-done(((bf16[16,3,128,128]{3,2,1,0:T(8,128)(2,1)}), bf16[16,3,128,128]{3,2,1,0:T(8,128)(2,1)S(1)}, u32[]{:S(2)}, u32[]{:S(2)}) %all-to-all-start) | async-done | bytes 1572896 | tf_op jit(solution)/shard_map/all_to_all | solution.py:306
  55.7 12.0 %attend.1.after = bf16[16,64,256]{2,1,0:T(8,128)(2,1)} custom-call(bf16[16,3,128,128]{3,2,1,0:T(8,128)(2,1)S(1)} %all-to-all-done.parts, bf16[4096,128]{1,0:T(8,128)(2,1)S(1)} %gate_columns.1.gate), custom_call_target="tpu_custom_call" | custom-call | flops 10000000000 | bytes 4000000 | tf_op jit(solution)/shard_map/attend/pallas_call | solution.py:175
  67.7 0.0 copy-done.3
  67.7 0.0 collective-permute-done.2.refs_3_
  67.7 0.0 collective-permute-done.1.refs_2_
  67.7 11.1 %collective-permute-done.refs_1_ = bf16[12,44,512]{2,1,0:T(8,128)(2,1)} collective-permute-done((bf16[12,44,512]{2,1,0:T(8,128)(2,1)S(1)}, bf16[12,44,512]{2,1,0:T(8,128)(2,1)}, u32[]{:S(2)}, u32[]{:S(2)}) %collective-permute-start) | collective-permute-done | bytes 540704 | tf_op jit(solution)/shard_map/ppermute | solution.py:314
  78.8 3.5 %assemble.1.mine = bf16[2112,512]{1,0:T(8,128)(2,1)} custom-call(s32[1]{0:T(128)} %bitcast.5.me, bf16[16,64,256]{2,1,0:T(8,128)(2,1)} %attend.1.after, bf16[12,44,512]{2,1,0:T(8,128)(2,1)} %copy-done.3, bf16[12,44,512]{2,1,0:T(8,128)(2,1)} %collective-permute-done.refs_1_, bf16[12,44,512]{2,1,0:T(8,128)(2,1)} %collective-permute-done.1.refs_2_, ...), custom_call_target="tpu_custom_call" | custom-call | flops 1000000 | bytes 4300000 | tf_op jit(solution)/shard_map/assemble/pallas_call | solution.py:212
  82.3 2.5 %collective-permute-start.3 = (bf16[2112,512]{1,0:T(8,128)(2,1)}, bf16[2112,512]{1,0:T(8,128)(2,1)S(1)}, u32[]{:S(2)}, u32[]{:S(2)}) collective-permute-start(bf16[2112,512]{1,0:T(8,128)(2,1)} %assemble.1.mine), channel_id=1, source_target_pairs={{0,48},{48,0},{1,49},{49,1},{2,50},{50,2},{3,51},{51,3},{4,52},{52... | collective-permute-start | bytes 6488072 | tf_op jit(solution)/shard_map/ppermute | solution.py:319
  84.8 7.1 %all-to-all-start.1 = ((bf16[16,64,256]{2,1,0:T(8,128)(2,1)}), bf16[16,64,256]{2,1,0:T(8,128)(2,1)S(1)}, u32[]{:S(2)}, u32[]{:S(2)}) async-start(bf16[16,64,256]{2,1,0:T(8,128)(2,1)} %attend.1.after), calls=%async_computation.1 | async-start | bytes 1048576 | tf_op jit(solution)/shard_map/all_to_all | solution.py:321
  91.9 0.0 collective-permute-done.3.source
  91.9 0.0 copy-start.2
  92.0 1.3 %copy-done.2 = bf16[2112,512]{1,0:T(8,128)(2,1)} copy-done((bf16[2112,512]{1,0:T(8,128)(2,1)}, bf16[2112,512]{1,0:T(8,128)(2,1)S(1)}, u32[]{:S(2)}) %copy-start.2) | copy-done | bytes 2162712
  93.3 15.9 %all-to-all-done.1.back = bf16[16,64,256]{2,1,0:T(8,128)(2,1)S(1)} async-done(((bf16[16,64,256]{2,1,0:T(8,128)(2,1)}), bf16[16,64,256]{2,1,0:T(8,128)(2,1)S(1)}, u32[]{:S(2)}, u32[]{:S(2)}) %all-to-all-start.1) | async-done | bytes 524320 | tf_op jit(solution)/shard_map/all_to_all | solution.py:321
  109.1 0.0 copy-start.4
  109.1 0.8 copy-done.4
  109.9 5.3 %project.1 = bf16[2112,256]{1,0:T(8,128)(2,1)} custom-call(s32[1]{0:T(128)} %bitcast.core, bf16[16,64,256]{2,1,0:T(8,128)(2,1)} %copy-done.4, bf16[2112,512]{1,0:T(8,128)(2,1)} %assemble.1.mine, bf16[2112,512]{1,0:T(8,128)(2,1)} %settle.1.other), custom_call_target="tpu_custom_call" | custom-call | flops 1100000000 | bytes 6000000 | tf_op jit(solution)/shard_map/project/pallas_call | solution.py:283
  (2 shorter events, 0.0 us)
Async XLA Ops:
  0.0 17.1 %copy-start = (bf16[1024,44]{0,1:T(8,128)(2,1)S(1)}, bf16[1024,44]{0,1:T(8,128)(2,1)}, u32[]{:S(2)}) copy-start(bf16[1024,44]{0,1:T(8,128)(2,1)} %param.9) | copy-start | bytes 270340
  3.1 49.4 %copy-start.1 = (f32[1,1,4096]{2,1,0:T(1,128)S(1)}, f32[1,1,4096]{2,1,0:T(1,128)}, u32[]{:S(2)}) copy-start(f32[1,1,4096]{2,1,0:T(1,128)} %param.8) | copy-start | bytes 49156
  3.1 52.6 %all-to-all-start = ((bf16[16,3,128,128]{3,2,1,0:T(8,128)(2,1)}), bf16[16,3,128,128]{3,2,1,0:T(8,128)(2,1)S(1)}, u32[]{:S(2)}, u32[]{:S(2)}) async-start(bf16[16,3,128,128]{3,2,1,0:T(8,128)(2,1)} %pack.1), calls=%async_computation | async-start | bytes 3145728 | tf_op jit(solution)/shard_map/all_to_all | solution.py:306
  43.2 24.6 %copy-start.3 = (bf16[12,44,512]{2,1,0:T(8,128)(2,1)}, bf16[12,44,512]{2,1,0:T(8,128)(2,1)S(1)}, u32[]{:S(2)}) copy-start(bf16[12,44,512]{2,1,0:T(8,128)(2,1)S(1)} %all-gather.1.refs_0_) | copy-start | bytes 1622020
  43.2 24.6 %collective-permute-start.2 = (bf16[12,44,512]{2,1,0:T(8,128)(2,1)S(1)}, bf16[12,44,512]{2,1,0:T(8,128)(2,1)}, u32[]{:S(2)}, u32[]{:S(2)}) collective-permute-start(bf16[12,44,512]{2,1,0:T(8,128)(2,1)S(1)} %all-gather.1.refs_0_), channel_id=1, source_target_pairs={{0,3},{1,0},{2,1},{3,2},{4,7},{5,4},{6,5},{7,6},{8,11},{9,8},{10,9... | collective-permute-start | bytes 1622024 | tf_op jit(solution)/shard_map/ppermute | solution.py:314
  47.6 20.2 %collective-permute-start.1 = (bf16[12,44,512]{2,1,0:T(8,128)(2,1)S(1)}, bf16[12,44,512]{2,1,0:T(8,128)(2,1)}, u32[]{:S(2)}, u32[]{:S(2)}) collective-permute-start(bf16[12,44,512]{2,1,0:T(8,128)(2,1)S(1)} %all-gather.1.refs_0_), channel_id=1, source_target_pairs={{0,2},{1,3},{2,0},{3,1},{4,6},{5,7},{6,4},{7,5},{8,10},{9,11},{10,... | collective-permute-start | bytes 1622024 | tf_op jit(solution)/shard_map/ppermute | solution.py:314
  50.0 28.8 %collective-permute-start = (bf16[12,44,512]{2,1,0:T(8,128)(2,1)S(1)}, bf16[12,44,512]{2,1,0:T(8,128)(2,1)}, u32[]{:S(2)}, u32[]{:S(2)}) collective-permute-start(bf16[12,44,512]{2,1,0:T(8,128)(2,1)S(1)} %all-gather.1.refs_0_), channel_id=1, source_target_pairs={{0,1},{1,2},{2,3},{3,0},{4,5},{5,6},{6,7},{7,4},{8,9},{9,10},{10,1... | collective-permute-start | bytes 1622024 | tf_op jit(solution)/shard_map/ppermute | solution.py:314
  82.3 9.6 %collective-permute-start.3 = (bf16[2112,512]{1,0:T(8,128)(2,1)}, bf16[2112,512]{1,0:T(8,128)(2,1)S(1)}, u32[]{:S(2)}, u32[]{:S(2)}) collective-permute-start(bf16[2112,512]{1,0:T(8,128)(2,1)} %assemble.1.mine), channel_id=1, source_target_pairs={{0,48},{48,0},{1,49},{49,1},{2,50},{50,2},{3,51},{51,3},{4,52},{52... | collective-permute-start | bytes 6488072 | tf_op jit(solution)/shard_map/ppermute | solution.py:319
  84.8 24.3 %all-to-all-start.1 = ((bf16[16,64,256]{2,1,0:T(8,128)(2,1)}), bf16[16,64,256]{2,1,0:T(8,128)(2,1)S(1)}, u32[]{:S(2)}, u32[]{:S(2)}) async-start(bf16[16,64,256]{2,1,0:T(8,128)(2,1)} %attend.1.after), calls=%async_computation.1 | async-start | bytes 1048576 | tf_op jit(solution)/shard_map/all_to_all | solution.py:321
  91.9 1.3 %copy-start.2 = (bf16[2112,512]{1,0:T(8,128)(2,1)}, bf16[2112,512]{1,0:T(8,128)(2,1)S(1)}, u32[]{:S(2)}) copy-start(bf16[2112,512]{1,0:T(8,128)(2,1)S(1)} %collective-permute-done.3.source) | copy-start | bytes 6488068
  109.1 0.8 copy-start.4

commit v5 on v3

--- a/solution.py
+++ b/solution.py
@@ -86,27 +86,29 @@
 
 def gate_kernel(gate, out):
     row = lax.broadcasted_iota(jnp.int32, (8, 128), 0)
-    for n in range(gate.shape[0]):
+
+    def split(n):
         g = jnp.broadcast_to(gate[n : n + 1, :] * -LOG2E, (8, 128))
         high = g.astype(jnp.bfloat16).astype(jnp.float32)
         rest = g - high
         middle = rest.astype(jnp.bfloat16).astype(jnp.float32)
         low = rest - middle
-        rows = jnp.where(row == 0, high, jnp.where(row == 1, middle, jnp.where(row == 2, low, 0.0)))
-        tile = jnp.concatenate(
-            [jnp.zeros((64, 128), jnp.float32), rows, jnp.zeros((56, 128), jnp.float32)], axis=0
-        )
-        out[128 * n : 128 * n + 128, :] = tile.T.astype(jnp.bfloat16)
+        return jnp.where(row == 0, high, jnp.where(row == 1, middle, jnp.where(row == 2, low, 0.0)))
+
+    empty = jnp.zeros((56, 128), jnp.float32)
+    for b in range(gate.shape[0] // 2):
+        tile = jnp.concatenate([split(2 * b + 1), empty, split(2 * b), empty], axis=0)
+        out[128 * b : 128 * b + 128, :] = tile.T.astype(jnp.bfloat16)
 
 
 def gate_columns(gate):
     return pl.pallas_call(
         gate_kernel,
-        out_shape=jax.ShapeDtypeStruct((gate.size, 128), jnp.bfloat16),
+        out_shape=jax.ShapeDtypeStruct((gate.size // 2, 128), jnp.bfloat16),
         in_specs=[VMEM],
         out_specs=VMEM,
-        cost_estimate=pl.CostEstimate(flops=10_000_000, bytes_accessed=1_000_000, transcendentals=0),
         compiler_params=pltpu.CompilerParams(vmem_limit_bytes=6 * 2**20),
+        cost_estimate=pl.CostEstimate(flops=10_000_000, bytes_accessed=500_000, transcendentals=0),
         name="gate_columns",
     )(gate)
 
@@ -121,10 +123,9 @@
         swapped = swap_halves(k)
         keys[base : base + 128, 0:128] = jnp.where(lanes, k, swapped)
         keys[base + 128 : base + 256, 0:128] = jnp.where(lanes, swapped, k)
-        keys[base : base + 128, 128:256] = jnp.where(lanes, k, gate[base : base + 128, :])
-        keys[base + 128 : base + 256, 128:256] = jnp.where(
-            lanes, swapped, gate[base + 128 : base + 256, :]
-        )
+        g = gate[128 * b : 128 * b + 128, :]
+        keys[base : base + 128, 128:256] = jnp.where(lanes, k, g)
+        keys[base + 128 : base + 256, 128:256] = jnp.where(lanes, swapped, swap_halves(g))
         v = parts[b, 2].T
         values[0:64, base : base + 128] = v[:64]
         values[0:64, base + 128 : base + 256] = v[64:]
@@ -220,31 +221,51 @@
     )(me, after, *blocks)
 
 
-def project_kernel(core, attended, mine, other, out):
+def project_kernel(core, attended, mine, source, out, other, partial, finished, arrived, left):
     heads, depth, rows = attended.shape
     c, half = core[0], heads // 2
+    steps = left.shape[0]
+    step = out.shape[0] // steps
+
+    def block(n):
+        return slice(step * n, step * n + step)
 
     def columns(first):
         return attended[pl.ds(first, half)].reshape(half * depth, rows)
 
-    total = jnp.dot(mine[...], columns(c * half), preferred_element_type=jnp.float32)
-    total += jnp.dot(other[...], columns((1 - c) * half), preferred_element_type=jnp.float32)
-    out[...] = total.astype(jnp.bfloat16)
+    def departure(n):
+        return pltpu.make_async_copy(finished.at[block(n)], out.at[block(n)], left.at[n])
+
+    arrival = pltpu.make_async_copy(source, other, arrived)
+    arrival.start()
+    partial[...] = jnp.dot(mine[...], columns(c * half), preferred_element_type=jnp.float32)
+    arrival.wait()
+    rest = columns((1 - c) * half)
+    for n in range(steps):
+        total = partial[block(n), :] + jnp.dot(
+            other[block(n), :], rest, preferred_element_type=jnp.float32
+        )
+        finished[block(n), :] = total.astype(jnp.bfloat16)
+        departure(n).start()
+    for n in range(steps):
+        departure(n).wait()
 
 
 def project(core, attended, mine, other):
-    columns, step = mine.shape[0], 352
+    columns, depth = mine.shape
+    rows, steps = attended.shape[2], 3
     return pl.pallas_call(
         project_kernel,
-        out_shape=jax.ShapeDtypeStruct((columns, attended.shape[2]), jnp.bfloat16),
-        grid=(columns // step,),
-        in_specs=[
-            SMEM,
-            pl.BlockSpec(attended.shape, lambda i: (0, 0, 0)),
-            pl.BlockSpec((step, mine.shape[1]), lambda i: (i, 0)),
-            pl.BlockSpec((step, other.shape[1]), lambda i: (i, 0)),
+        out_shape=jax.ShapeDtypeStruct((columns, rows), jnp.bfloat16),
+        in_specs=[SMEM, VMEM, VMEM, HBM],
+        out_specs=HBM,
+        scratch_shapes=[
+            pltpu.VMEM((columns, depth), jnp.bfloat16),
+            pltpu.VMEM((columns, rows), jnp.float32),
+            pltpu.VMEM((columns, rows), jnp.bfloat16),
+            pltpu.SemaphoreType.DMA,
+            pltpu.SemaphoreType.DMA((steps,)),
         ],
-        out_specs=pl.BlockSpec((step, attended.shape[2]), lambda i: (i, 0)),
         compiler_params=pltpu.CompilerParams(vmem_limit_bytes=16 * 2**20),
         cost_estimate=pl.CostEstimate(
             flops=1_100_000_000, bytes_accessed=6_000_000, transcendentals=0

time: 109 us -> 109 us (level)
  local copies, waits for them, and re-layouts: 0.02 us -> 1.85 us
  waiting for transfers between devices: 9.34 us -> 7.59 us
    unnamed x5 -> x9, local copies, waits for them, and re-layouts: 0.02 us -> 1.85 us
where the time goes in v5:
time: 109 us
  blocking collectives  50.3 us (46%)
  starting transfers between devices  29.1 us (27%)
  Pallas kernels  19.7 us (18%)
  waiting for transfers between devices  7.59 us (7%)
  local copies, waits for them, and re-layouts  1.85 us (2%)
    all_gather x1, blocking collectives, body(): along_z = lax.all_gather(own[None], 'z', axis=0, tiled=True)  26 us
    all_to_all x1, blocking collectives, body(): back = lax.all_to_all(local, SP, 0, 0, tiled=True)  24.2 us
    all_to_all x1, starting transfers between devices, body(): parts = lax.all_to_all(packed, SP, 0, 0, tiled=True)  14 us
    pallas_call x1, Pallas kernels, attend(): pl.pallas_call(attend_kernel, out_shape=jax.ShapeDtypeStruct((count, 64,...  11.3 us
    ppermute x3, starting transfers between devices, body(): lax.ppermute(along_z, 'x', [(i, (i + hop) % n) for i in range(n)])  10.5 us
    ppermute x3, waiting for transfers between devices, body(): lax.ppermute(along_z, 'x', [(i, (i + hop) % n) for i in range(n)])  6.64 us
    ppermute x1, starting transfers between devices, body(): other = lax.ppermute(mine, 'sp_1', [(0, 1), (1, 0)])  4.55 us
    pallas_call x1, Pallas kernels, project(): pl.pallas_call(project_kernel, out_shape=jax.ShapeDtypeStruct((columns, r...  3.54 us
  transfers between devices with their start and end apart: 5, of which 3 were waited for; matrix products, arithmetic and copies ran while one was open for 0% of the time, Pallas kernels for 11%

profile of v5, /device:TPU:1, one launch (start us, length us, event | category | flops | bytes accessed | tf_op | source)
XLA Modules:
  0.0 108.6 jit_solution(12549223451464722621)
XLA Ops:
  0.0 0.0 copy-start
  0.0 3.1 %pack.1 = bf16[16,3,128,128]{3,2,1,0:T(8,128)(2,1)} custom-call(bf16[256,1024]{1,0:T(8,128)(2,1)} %bitcast.14, bf16[256,1024]{1,0:T(8,128)(2,1)} %bitcast.15, bf16[256,1024]{1,0:T(8,128)(2,1)} %bitcast.16), custom_call_target="tpu_custom_call" | custom-call | flops 1000000 | bytes 3000000 | tf_op jit(solution)/shard_map/pack/pallas_call | solution.py:70
  3.1 0.0 copy-start.3
  3.1 14.0 %all-to-all-start = ((bf16[16,3,128,128]{3,2,1,0:T(8,128)(2,1)}), bf16[16,3,128,128]{3,2,1,0:T(8,128)(2,1)S(1)}, u32[]{:S(2)}, u32[]{:S(2)}) async-start(bf16[16,3,128,128]{3,2,1,0:T(8,128)(2,1)} %pack.1), calls=%async_computation | async-start | bytes 3145728 | tf_op jit(solution)/shard_map/all_to_all | solution.py:280
  17.1 0.0 copy-done
  17.1 26.0 %all-gather.1.refs_0_ = bf16[12,44,512]{2,1,0:T(8,128)(2,1)S(1)} all-gather(bf16[1,44,512]{2,1,0:T(8,128)(2,1)S(1)} %dynamic-slice_bitcast_fusion), channel_id=2, replica_groups=mesh['sp_0'=8,'sp_1'=2,'z'=12,'x'=4] {'z'}, dimensions={0}, use_global_device_ids=true | all-gather | bytes 585728 | tf_op jit(solution)/shard_map/all_gather | solution.py:285
  43.2 3.1 %collective-permute-start = (bf16[12,44,512]{2,1,0:T(8,128)(2,1)S(1)}, bf16[12,44,512]{2,1,0:T(8,128)(2,1)S(1)}, u32[]{:S(2)}, u32[]{:S(2)}) collective-permute-start(bf16[12,44,512]{2,1,0:T(8,128)(2,1)S(1)} %all-gather.1.refs_0_), channel_id=1, source_target_pairs={{0,1},{1,2},{2,3},{3,0},{4,5},{5,6},{6,7},{7,4},{8,9},{9,10},{10,1... | collective-permute-start | bytes 1622024 | tf_op jit(solution)/shard_map/ppermute | solution.py:288
  46.3 4.4 %collective-permute-start.1 = (bf16[12,44,512]{2,1,0:T(8,128)(2,1)S(1)}, bf16[12,44,512]{2,1,0:T(8,128)(2,1)S(1)}, u32[]{:S(2)}, u32[]{:S(2)}) collective-permute-start(bf16[12,44,512]{2,1,0:T(8,128)(2,1)S(1)} %all-gather.1.refs_0_), channel_id=1, source_target_pairs={{0,2},{1,3},{2,0},{3,1},{4,6},{5,7},{6,4},{7,5},{8,10},{9,11},{10,... | collective-permute-start | bytes 1622024 | tf_op jit(solution)/shard_map/ppermute | solution.py:288
  50.6 3.1 %collective-permute-start.2 = (bf16[12,44,512]{2,1,0:T(8,128)(2,1)S(1)}, bf16[12,44,512]{2,1,0:T(8,128)(2,1)}, u32[]{:S(2)}, u32[]{:S(2)}) collective-permute-start(bf16[12,44,512]{2,1,0:T(8,128)(2,1)S(1)} %all-gather.1.refs_0_), channel_id=1, source_target_pairs={{0,3},{1,0},{2,1},{3,2},{4,7},{5,4},{6,5},{7,6},{8,11},{9,8},{10,9... | collective-permute-start | bytes 1622024 | tf_op jit(solution)/shard_map/ppermute | solution.py:288
  53.7 0.0 copy-done.3
  53.7 0.2 gate_columns.1.gate
  54.0 0.0 copy-start.1
  54.0 0.8 copy-done.1
  54.7 0.9 all-to-all-done.parts
  55.7 0.0 copy-start.2
  55.7 1.0 copy-done.2
  56.7 11.3 %attend.1.after = bf16[16,64,256]{2,1,0:T(8,128)(2,1)S(1)} custom-call(bf16[16,3,128,128]{3,2,1,0:T(8,128)(2,1)S(1)} %all-to-all-done.parts, bf16[2048,128]{1,0:T(8,128)(2,1)S(1)} %copy-done.2), custom_call_target="tpu_custom_call" | custom-call | flops 10000000000 | bytes 4000000 | tf_op jit(solution)/shard_map/attend/pallas_call | solution.py:176
  68.0 0.0 collective-permute-done.refs_1_
  68.0 2.1 %collective-permute-done.1.refs_2_ = bf16[12,44,512]{2,1,0:T(8,128)(2,1)S(1)} collective-permute-done((bf16[12,44,512]{2,1,0:T(8,128)(2,1)S(1)}, bf16[12,44,512]{2,1,0:T(8,128)(2,1)S(1)}, u32[]{:S(2)}, u32[]{:S(2)}) %collective-permute-start.1) | collective-permute-done | bytes 540704 | tf_op jit(solution)/shard_map/ppermute | solution.py:288
  70.2 4.5 %collective-permute-done.2.refs_3_ = bf16[12,44,512]{2,1,0:T(8,128)(2,1)} collective-permute-done((bf16[12,44,512]{2,1,0:T(8,128)(2,1)S(1)}, bf16[12,44,512]{2,1,0:T(8,128)(2,1)}, u32[]{:S(2)}, u32[]{:S(2)}) %collective-permute-start.2) | collective-permute-done | bytes 540704 | tf_op jit(solution)/shard_map/ppermute | solution.py:288
  74.6 1.6 %assemble.1.mine = bf16[2112,512]{1,0:T(8,128)(2,1)S(1)} custom-call(s32[1]{0:T(128)} %bitcast.5.me, bf16[16,64,256]{2,1,0:T(8,128)(2,1)S(1)} %attend.1.after, bf16[12,44,512]{2,1,0:T(8,128)(2,1)S(1)} %all-gather.1.refs_0_, bf16[12,44,512]{2,1,0:T(8,128)(2,1)S(1)} %collective-permute-done.refs_1_, bf16[12,44,512]{2,1,0:T(8,128)(2,1)S(1)} %collective-permute-done.1.refs_2_, ...), custom_call_target="tpu_custom_call" | custom-call | flops 1000000 | bytes 4300000 | tf_op jit(solution)/shard_map/assemble/pallas_call | solution.py:213
  76.3 4.5 %collective-permute-start.3 = (bf16[2112,512]{1,0:T(8,128)(2,1)S(1)}, bf16[2112,512]{1,0:T(8,128)(2,1)S(1)}, u32[]{:S(2)}, u32[]{:S(2)}) collective-permute-start(bf16[2112,512]{1,0:T(8,128)(2,1)S(1)} %assemble.1.mine), channel_id=1, source_target_pairs={{0,48},{48,0},{1,49},{49,1},{2,50},{50,2},{3,51},{51,3},{4,52},{52... | collective-permute-start | bytes 6488072 | tf_op jit(solution)/shard_map/ppermute | solution.py:293
  80.8 24.2 %all_to_all.10.attended = bf16[16,64,256]{2,1,0:T(8,128)(2,1)S(1)} all-to-all(bf16[16,64,256]{2,1,0:T(8,128)(2,1)S(1)} %attend.1.after), channel_id=1, replica_groups=mesh['sp_0'=8,'sp_1'=2,'z'=12,'x'=4] {'sp_0','sp_1'}, dimensions={0} | all-to-all | bytes 1048576 | tf_op jit(solution)/shard_map/all_to_all | solution.py:294
  105.1 0.0 collective-permute-done.3.source
  105.1 3.5 %project.1 = bf16[2112,256]{1,0:T(8,128)(2,1)} custom-call(s32[1]{0:T(128)} %bitcast.core, bf16[16,64,256]{2,1,0:T(8,128)(2,1)S(1)} %all_to_all.10.attended, bf16[2112,512]{1,0:T(8,128)(2,1)S(1)} %assemble.1.mine, bf16[2112,512]{1,0:T(8,128)(2,1)S(1)} %collective-permute-done.3.source), custom_call_target="tpu_custom_call" | custom-call | flops 1100000000 | bytes 6000000 | tf_op jit(solution)/shard_map/project/pallas_call | solution.py:257
  (1 shorter events, 0.0 us)
Async XLA Ops:
  0.0 17.1 %copy-start = (bf16[1024,44]{0,1:T(8,128)(2,1)S(1)}, bf16[1024,44]{0,1:T(8,128)(2,1)}, u32[]{:S(2)}) copy-start(bf16[1024,44]{0,1:T(8,128)(2,1)} %param.9) | copy-start | bytes 270340
  3.1 50.6 %copy-start.3 = (f32[1,1,4096]{2,1,0:T(1,128)S(1)}, f32[1,1,4096]{2,1,0:T(1,128)}, u32[]{:S(2)}) copy-start(f32[1,1,4096]{2,1,0:T(1,128)} %param.8) | copy-start | bytes 49156
  3.1 52.6 %all-to-all-start = ((bf16[16,3,128,128]{3,2,1,0:T(8,128)(2,1)}), bf16[16,3,128,128]{3,2,1,0:T(8,128)(2,1)S(1)}, u32[]{:S(2)}, u32[]{:S(2)}) async-start(bf16[16,3,128,128]{3,2,1,0:T(8,128)(2,1)} %pack.1), calls=%async_computation | async-start | bytes 3145728 | tf_op jit(solution)/shard_map/all_to_all | solution.py:280
  43.2 24.8 %collective-permute-start = (bf16[12,44,512]{2,1,0:T(8,128)(2,1)S(1)}, bf16[12,44,512]{2,1,0:T(8,128)(2,1)S(1)}, u32[]{:S(2)}, u32[]{:S(2)}) collective-permute-start(bf16[12,44,512]{2,1,0:T(8,128)(2,1)S(1)} %all-gather.1.refs_0_), channel_id=1, source_target_pairs={{0,1},{1,2},{2,3},{3,0},{4,5},{5,6},{6,7},{7,4},{8,9},{9,10},{10,1... | collective-permute-start | bytes 1622024 | tf_op jit(solution)/shard_map/ppermute | solution.py:288
  46.3 23.9 %collective-permute-start.1 = (bf16[12,44,512]{2,1,0:T(8,128)(2,1)S(1)}, bf16[12,44,512]{2,1,0:T(8,128)(2,1)S(1)}, u32[]{:S(2)}, u32[]{:S(2)}) collective-permute-start(bf16[12,44,512]{2,1,0:T(8,128)(2,1)S(1)} %all-gather.1.refs_0_), channel_id=1, source_target_pairs={{0,2},{1,3},{2,0},{3,1},{4,6},{5,7},{6,4},{7,5},{8,10},{9,11},{10,... | collective-permute-start | bytes 1622024 | tf_op jit(solution)/shard_map/ppermute | solution.py:288
  50.6 24.0 %collective-permute-start.2 = (bf16[12,44,512]{2,1,0:T(8,128)(2,1)S(1)}, bf16[12,44,512]{2,1,0:T(8,128)(2,1)}, u32[]{:S(2)}, u32[]{:S(2)}) collective-permute-start(bf16[12,44,512]{2,1,0:T(8,128)(2,1)S(1)} %all-gather.1.refs_0_), channel_id=1, source_target_pairs={{0,3},{1,0},{2,1},{3,2},{4,7},{5,4},{6,5},{7,6},{8,11},{9,8},{10,9... | collective-permute-start | bytes 1622024 | tf_op jit(solution)/shard_map/ppermute | solution.py:288
  54.0 0.8 copy-start.1
  55.7 1.0 copy-start.2
  76.3 28.8 %collective-permute-start.3 = (bf16[2112,512]{1,0:T(8,128)(2,1)S(1)}, bf16[2112,512]{1,0:T(8,128)(2,1)S(1)}, u32[]{:S(2)}, u32[]{:S(2)}) collective-permute-start(bf16[2112,512]{1,0:T(8,128)(2,1)S(1)} %assemble.1.mine), channel_id=1, source_target_pairs={{0,48},{48,0},{1,49},{49,1},{2,50},{50,2},{3,51},{51,3},{4,52},{52... | collective-permute-start | bytes 6488072 | tf_op jit(solution)/shard_map/ppermute | solution.py:293

commit v6 on v5

--- a/solution.py
+++ b/solution.py
@@ -221,7 +221,7 @@
     )(me, after, *blocks)
 
 
-def project_kernel(core, attended, mine, source, out, other, partial, finished, arrived, left):
+def project_kernel(core, attended, mine, other, out, finished, left):
     heads, depth, rows = attended.shape
     c, half = core[0], heads // 2
     steps = left.shape[0]
@@ -236,15 +236,10 @@
     def departure(n):
         return pltpu.make_async_copy(finished.at[block(n)], out.at[block(n)], left.at[n])
 
-    arrival = pltpu.make_async_copy(source, other, arrived)
-    arrival.start()
-    partial[...] = jnp.dot(mine[...], columns(c * half), preferred_element_type=jnp.float32)
-    arrival.wait()
-    rest = columns((1 - c) * half)
+    own, rest = columns(c * half), columns((1 - c) * half)
     for n in range(steps):
-        total = partial[block(n), :] + jnp.dot(
-            other[block(n), :], rest, preferred_element_type=jnp.float32
-        )
+        total = jnp.dot(mine[block(n), :], own, preferred_element_type=jnp.float32)
+        total += jnp.dot(other[block(n), :], rest, preferred_element_type=jnp.float32)
         finished[block(n), :] = total.astype(jnp.bfloat16)
         departure(n).start()
     for n in range(steps):
@@ -252,18 +247,15 @@
 
 
 def project(core, attended, mine, other):
-    columns, depth = mine.shape
-    rows, steps = attended.shape[2], 3
+    columns, _ = mine.shape
+    rows, steps = attended.shape[2], 4
     return pl.pallas_call(
         project_kernel,
         out_shape=jax.ShapeDtypeStruct((columns, rows), jnp.bfloat16),
-        in_specs=[SMEM, VMEM, VMEM, HBM],
+        in_specs=[SMEM, VMEM, VMEM, VMEM],
         out_specs=HBM,
         scratch_shapes=[
-            pltpu.VMEM((columns, depth), jnp.bfloat16),
-            pltpu.VMEM((columns, rows), jnp.float32),
             pltpu.VMEM((columns, rows), jnp.bfloat16),
-            pltpu.SemaphoreType.DMA,
             pltpu.SemaphoreType.DMA((steps,)),
         ],
         compiler_params=pltpu.CompilerParams(vmem_limit_bytes=16 * 2**20),

time: 109 us -> 108 us (level)
  Pallas kernels: 19.7 us -> 18.3 us
    pallas_call x1, Pallas kernels: 3.54 us -> 2.14 us  [project(): pl.pallas_call(project_kernel, out_shape=jax.ShapeDtypeStruct((columns, r...]
where the time goes in v6:
time: 108 us; the launch traced here: 107 us
  blocking collectives  50.3 us (47%)
  starting transfers between devices  29.1 us (27%)
  Pallas kernels  18.3 us (17%)
  waiting for transfers between devices  7.59 us (7%)
  local copies, waits for them, and re-layouts  1.85 us (2%)
    all_gather x1, blocking collectives, body(): along_z = lax.all_gather(own[None], 'z', axis=0, tiled=True)  26 us
    all_to_all x1, blocking collectives, body(): back = lax.all_to_all(local, SP, 0, 0, tiled=True)  24.2 us
    all_to_all x1, starting transfers between devices, body(): parts = lax.all_to_all(packed, SP, 0, 0, tiled=True)  14 us
    pallas_call x1, Pallas kernels, attend(): pl.pallas_call(attend_kernel, out_shape=jax.ShapeDtypeStruct((count, 64,...  11.3 us
    ppermute x3, starting transfers between devices, body(): lax.ppermute(along_z, 'x', [(i, (i + hop) % n) for i in range(n)])  10.5 us
    ppermute x3, waiting for transfers between devices, body(): lax.ppermute(along_z, 'x', [(i, (i + hop) % n) for i in range(n)])  6.64 us
    ppermute x1, starting transfers between devices, body(): other = lax.ppermute(mine, 'sp_1', [(0, 1), (1, 0)])  4.55 us
    pallas_call x1, Pallas kernels, pack(): pl.pallas_call(pack_kernel, out_shape=jax.ShapeDtypeStruct((heads, 3, row...  3.11 us
  transfers between devices with their start and end apart: 5, of which 3 were waited for; matrix products, arithmetic and copies ran while one was open for 0% of the time, Pallas kernels for 11%

profile of v6, /device:TPU:1, one launch (start us, length us, event | category | flops | bytes accessed | tf_op | source)
XLA Modules:
  0.0 107.2 jit_solution(15694489254717176634)
XLA Ops:
  0.0 0.0 copy-start
  0.0 3.1 %pack.1 = bf16[16,3,128,128]{3,2,1,0:T(8,128)(2,1)} custom-call(bf16[256,1024]{1,0:T(8,128)(2,1)} %bitcast.14, bf16[256,1024]{1,0:T(8,128)(2,1)} %bitcast.15, bf16[256,1024]{1,0:T(8,128)(2,1)} %bitcast.16), custom_call_target="tpu_custom_call" | custom-call | flops 1000000 | bytes 3000000 | tf_op jit(solution)/shard_map/pack/pallas_call | solution.py:70
  3.1 0.0 copy-start.3
  3.1 14.0 %all-to-all-start = ((bf16[16,3,128,128]{3,2,1,0:T(8,128)(2,1)}), bf16[16,3,128,128]{3,2,1,0:T(8,128)(2,1)S(1)}, u32[]{:S(2)}, u32[]{:S(2)}) async-start(bf16[16,3,128,128]{3,2,1,0:T(8,128)(2,1)} %pack.1), calls=%async_computation | async-start | bytes 3145728 | tf_op jit(solution)/shard_map/all_to_all | solution.py:272
  17.1 0.0 copy-done
  17.1 26.0 %all-gather.1.refs_0_ = bf16[12,44,512]{2,1,0:T(8,128)(2,1)S(1)} all-gather(bf16[1,44,512]{2,1,0:T(8,128)(2,1)S(1)} %dynamic-slice_bitcast_fusion), channel_id=2, replica_groups=mesh['sp_0'=8,'sp_1'=2,'z'=12,'x'=4] {'z'}, dimensions={0}, use_global_device_ids=true | all-gather | bytes 585728 | tf_op jit(solution)/shard_map/all_gather | solution.py:277
  43.2 3.1 %collective-permute-start = (bf16[12,44,512]{2,1,0:T(8,128)(2,1)S(1)}, bf16[12,44,512]{2,1,0:T(8,128)(2,1)S(1)}, u32[]{:S(2)}, u32[]{:S(2)}) collective-permute-start(bf16[12,44,512]{2,1,0:T(8,128)(2,1)S(1)} %all-gather.1.refs_0_), channel_id=1, source_target_pairs={{0,1},{1,2},{2,3},{3,0},{4,5},{5,6},{6,7},{7,4},{8,9},{9,10},{10,1... | collective-permute-start | bytes 1622024 | tf_op jit(solution)/shard_map/ppermute | solution.py:280
  46.3 4.4 %collective-permute-start.1 = (bf16[12,44,512]{2,1,0:T(8,128)(2,1)S(1)}, bf16[12,44,512]{2,1,0:T(8,128)(2,1)S(1)}, u32[]{:S(2)}, u32[]{:S(2)}) collective-permute-start(bf16[12,44,512]{2,1,0:T(8,128)(2,1)S(1)} %all-gather.1.refs_0_), channel_id=1, source_target_pairs={{0,2},{1,3},{2,0},{3,1},{4,6},{5,7},{6,4},{7,5},{8,10},{9,11},{10,... | collective-permute-start | bytes 1622024 | tf_op jit(solution)/shard_map/ppermute | solution.py:280
  50.6 3.1 %collective-permute-start.2 = (bf16[12,44,512]{2,1,0:T(8,128)(2,1)S(1)}, bf16[12,44,512]{2,1,0:T(8,128)(2,1)}, u32[]{:S(2)}, u32[]{:S(2)}) collective-permute-start(bf16[12,44,512]{2,1,0:T(8,128)(2,1)S(1)} %all-gather.1.refs_0_), channel_id=1, source_target_pairs={{0,3},{1,0},{2,1},{3,2},{4,7},{5,4},{6,5},{7,6},{8,11},{9,8},{10,9... | collective-permute-start | bytes 1622024 | tf_op jit(solution)/shard_map/ppermute | solution.py:280
  53.7 0.0 copy-done.3
  53.7 0.2 gate_columns.1.gate
  54.0 0.0 copy-start.1
  54.0 0.8 copy-done.1
  54.7 0.9 all-to-all-done.parts
  55.7 0.0 copy-start.2
  55.7 1.0 copy-done.2
  56.7 11.3 %attend.1.after = bf16[16,64,256]{2,1,0:T(8,128)(2,1)S(1)} custom-call(bf16[16,3,128,128]{3,2,1,0:T(8,128)(2,1)S(1)} %all-to-all-done.parts, bf16[2048,128]{1,0:T(8,128)(2,1)S(1)} %copy-done.2), custom_call_target="tpu_custom_call" | custom-call | flops 10000000000 | bytes 4000000 | tf_op jit(solution)/shard_map/attend/pallas_call | solution.py:176
  68.0 0.0 collective-permute-done.refs_1_
  68.0 2.1 %collective-permute-done.1.refs_2_ = bf16[12,44,512]{2,1,0:T(8,128)(2,1)S(1)} collective-permute-done((bf16[12,44,512]{2,1,0:T(8,128)(2,1)S(1)}, bf16[12,44,512]{2,1,0:T(8,128)(2,1)S(1)}, u32[]{:S(2)}, u32[]{:S(2)}) %collective-permute-start.1) | collective-permute-done | bytes 540704 | tf_op jit(solution)/shard_map/ppermute | solution.py:280
  70.2 4.5 %collective-permute-done.2.refs_3_ = bf16[12,44,512]{2,1,0:T(8,128)(2,1)} collective-permute-done((bf16[12,44,512]{2,1,0:T(8,128)(2,1)S(1)}, bf16[12,44,512]{2,1,0:T(8,128)(2,1)}, u32[]{:S(2)}, u32[]{:S(2)}) %collective-permute-start.2) | collective-permute-done | bytes 540704 | tf_op jit(solution)/shard_map/ppermute | solution.py:280
  74.6 1.6 %assemble.1.mine = bf16[2112,512]{1,0:T(8,128)(2,1)S(1)} custom-call(s32[1]{0:T(128)} %bitcast.5.me, bf16[16,64,256]{2,1,0:T(8,128)(2,1)S(1)} %attend.1.after, bf16[12,44,512]{2,1,0:T(8,128)(2,1)S(1)} %all-gather.1.refs_0_, bf16[12,44,512]{2,1,0:T(8,128)(2,1)S(1)} %collective-permute-done.refs_1_, bf16[12,44,512]{2,1,0:T(8,128)(2,1)S(1)} %collective-permute-done.1.refs_2_, ...), custom_call_target="tpu_custom_call" | custom-call | flops 1000000 | bytes 4300000 | tf_op jit(solution)/shard_map/assemble/pallas_call | solution.py:213
  76.3 4.5 %collective-permute-start.3 = (bf16[2112,512]{1,0:T(8,128)(2,1)S(1)}, bf16[2112,512]{1,0:T(8,128)(2,1)S(1)}, u32[]{:S(2)}, u32[]{:S(2)}) collective-permute-start(bf16[2112,512]{1,0:T(8,128)(2,1)S(1)} %assemble.1.mine), channel_id=1, source_target_pairs={{0,48},{48,0},{1,49},{49,1},{2,50},{50,2},{3,51},{51,3},{4,52},{52... | collective-permute-start | bytes 6488072 | tf_op jit(solution)/shard_map/ppermute | solution.py:285
  80.8 24.2 %all_to_all.10.attended = bf16[16,64,256]{2,1,0:T(8,128)(2,1)S(1)} all-to-all(bf16[16,64,256]{2,1,0:T(8,128)(2,1)S(1)} %attend.1.after), channel_id=1, replica_groups=mesh['sp_0'=8,'sp_1'=2,'z'=12,'x'=4] {'sp_0','sp_1'}, dimensions={0} | all-to-all | bytes 1048576 | tf_op jit(solution)/shard_map/all_to_all | solution.py:286
  105.1 0.0 collective-permute-done.3.other
  105.1 2.1 %project.1 = bf16[2112,256]{1,0:T(8,128)(2,1)} custom-call(s32[1]{0:T(128)} %bitcast.core, bf16[16,64,256]{2,1,0:T(8,128)(2,1)S(1)} %all_to_all.10.attended, bf16[2112,512]{1,0:T(8,128)(2,1)S(1)} %assemble.1.mine, bf16[2112,512]{1,0:T(8,128)(2,1)S(1)} %collective-permute-done.3.other), custom_call_target="tpu_custom_call" | custom-call | flops 1100000000 | bytes 6000000 | tf_op jit(solution)/shard_map/project/pallas_call | solution.py:252
  (1 shorter events, 0.0 us)
Async XLA Ops:
  0.0 17.1 %copy-start = (bf16[1024,44]{0,1:T(8,128)(2,1)S(1)}, bf16[1024,44]{0,1:T(8,128)(2,1)}, u32[]{:S(2)}) copy-start(bf16[1024,44]{0,1:T(8,128)(2,1)} %param.9) | copy-start | bytes 270340
  3.1 50.6 %copy-start.3 = (f32[1,1,4096]{2,1,0:T(1,128)S(1)}, f32[1,1,4096]{2,1,0:T(1,128)}, u32[]{:S(2)}) copy-start(f32[1,1,4096]{2,1,0:T(1,128)} %param.8) | copy-start | bytes 49156
  3.1 52.6 %all-to-all-start = ((bf16[16,3,128,128]{3,2,1,0:T(8,128)(2,1)}), bf16[16,3,128,128]{3,2,1,0:T(8,128)(2,1)S(1)}, u32[]{:S(2)}, u32[]{:S(2)}) async-start(bf16[16,3,128,128]{3,2,1,0:T(8,128)(2,1)} %pack.1), calls=%async_computation | async-start | bytes 3145728 | tf_op jit(solution)/shard_map/all_to_all | solution.py:272
  43.2 24.8 %collective-permute-start = (bf16[12,44,512]{2,1,0:T(8,128)(2,1)S(1)}, bf16[12,44,512]{2,1,0:T(8,128)(2,1)S(1)}, u32[]{:S(2)}, u32[]{:S(2)}) collective-permute-start(bf16[12,44,512]{2,1,0:T(8,128)(2,1)S(1)} %all-gather.1.refs_0_), channel_id=1, source_target_pairs={{0,1},{1,2},{2,3},{3,0},{4,5},{5,6},{6,7},{7,4},{8,9},{9,10},{10,1... | collective-permute-start | bytes 1622024 | tf_op jit(solution)/shard_map/ppermute | solution.py:280
  46.3 23.9 %collective-permute-start.1 = (bf16[12,44,512]{2,1,0:T(8,128)(2,1)S(1)}, bf16[12,44,512]{2,1,0:T(8,128)(2,1)S(1)}, u32[]{:S(2)}, u32[]{:S(2)}) collective-permute-start(bf16[12,44,512]{2,1,0:T(8,128)(2,1)S(1)} %all-gather.1.refs_0_), channel_id=1, source_target_pairs={{0,2},{1,3},{2,0},{3,1},{4,6},{5,7},{6,4},{7,5},{8,10},{9,11},{10,... | collective-permute-start | bytes 1622024 | tf_op jit(solution)/shard_map/ppermute | solution.py:280
  50.6 24.0 %collective-permute-start.2 = (bf16[12,44,512]{2,1,0:T(8,128)(2,1)S(1)}, bf16[12,44,512]{2,1,0:T(8,128)(2,1)}, u32[]{:S(2)}, u32[]{:S(2)}) collective-permute-start(bf16[12,44,512]{2,1,0:T(8,128)(2,1)S(1)} %all-gather.1.refs_0_), channel_id=1, source_target_pairs={{0,3},{1,0},{2,1},{3,2},{4,7},{5,4},{6,5},{7,6},{8,11},{9,8},{10,9... | collective-permute-start | bytes 1622024 | tf_op jit(solution)/shard_map/ppermute | solution.py:280
  54.0 0.8 copy-start.1
  55.7 1.0 copy-start.2
  76.3 28.8 %collective-permute-start.3 = (bf16[2112,512]{1,0:T(8,128)(2,1)S(1)}, bf16[2112,512]{1,0:T(8,128)(2,1)S(1)}, u32[]{:S(2)}, u32[]{:S(2)}) collective-permute-start(bf16[2112,512]{1,0:T(8,128)(2,1)S(1)} %assemble.1.mine), channel_id=1, source_target_pairs={{0,48},{48,0},{1,49},{49,1},{2,50},{50,2},{3,51},{51,3},{4,52},{52... | collective-permute-start | bytes 6488072 | tf_op jit(solution)/shard_map/ppermute | solution.py:285
